TPU v7x, 512 devices: a whole 4x4x16 slice. The times are simulated.
512 devices in a mesh: sp: 64 (over z, y), tp: 8 (over x, core).
Axes of the slice: x: 4, y: 4, z: 16, core: 2. Of those that a mesh axis runs over, the one named last changes fastest.
Arguments:
- receptance: bfloat16 [12288, 1024], P('sp', 'tp'), may hold values from -6 to 6
- head_keys: bfloat16 [12288, 1024], P('sp', 'tp'), may hold values from -6 to 6
- head_values: bfloat16 [12288, 1024], P('sp', 'tp'), may hold values from -6 to 6
- decay_preact: float32 [12288, 1024], P('sp', 'tp'), may hold values from -13.5 to -0.5
- learning_rate_preact: float32 [12288, 1024], P('sp', 'tp'), may hold values from -10.5 to 2.5
- output_gate_preact: bfloat16 [12288, 1024], P('sp', 'tp'), may hold values from -8 to 8
- self_token_weight: float32 [16, 64], P('tp'), may hold values from -0.6 to 0.6
- head_norm_gain: float32 [1024], P('tp'), may hold values from 0.1 to 1.9
- output_weight: bfloat16 [1024, 2048], P('tp'), may hold values from -0.1875 to 0.1875
- residual: bfloat16 [12288, 2048], P('sp'), may hold values from -6 to 6
- premixer_norm_gain: float32 [2048], replicated, may hold values from 0.1 to 1.9
- mixer_gate_weight: bfloat16 [2048, 5120], P('sp', 'tp'), may hold values from -0.125 to 0.125
- mixer_up_weight: bfloat16 [2048, 5120], P('sp', 'tp'), may hold values from -0.125 to 0.125
- mixer_down_weight: bfloat16 [5120, 2048], P('tp', 'sp'), may hold values from -0.078125 to 0.078125
Outputs:
- layer_out: bfloat16 [12288, 2048], P(('sp', 'tp'))
All inputs are finite; a program needn't handle non-finite values.
Results may differ from a plain program's by a relative error of at most 0.015.
Values may be sent and summed in bfloat16 or wider, within the bound.
A program may use at most 64 MiB of HBM per device.

v0:
```python
import jax
import jax.numpy as jnp
from jax import lax
from jax.sharding import Mesh
from jax.sharding import PartitionSpec as P

HEAD_SIZE = 64
SUB = 16
SP = ("sp_0", "sp_1")
SP_TP = ("sp_0", "sp_1", "tp")


GROUP_EPS = 0.00064
NORM_EPS = 1e-06
EXACT = lax.Precision.HIGHEST


def neutral_like(x, identity):
    return jax.tree.map(
        lambda part, zero: jnp.zeros_like(part) + jnp.asarray(zero, part.dtype), x, identity
    )


def gathered_once(x, axis):
    leaves = jax.tree.leaves(x)
    turns = sorted(range(len(leaves)), key=lambda k: -leaves[k].size)
    width = (1, *leaves[turns[0]].shape)[-1]
    lines = [
        jnp.pad(leaves[k].reshape(-1), (0, -leaves[k].size % width)).reshape(-1, width)
        for k in turns
    ]
    both, at, found = (lax.all_gather(jnp.concatenate(lines), axis), 0, {})
    for k, line in zip(turns, lines):
        piece = both[:, at : at + len(line)].reshape(len(both), -1)
        found[k] = piece[:, : leaves[k].size].reshape(-1, *leaves[k].shape)
        at += len(line)
    numbers = iter(range(len(leaves)))
    return jax.tree.map(lambda _: found[next(numbers)], x)


def entering(x, axes, combine, identity):
    before = start = neutral_like(x, identity)
    running = x
    for axis in reversed(axes):
        length, here = (lax.axis_size(axis), lax.axis_index(axis))
        pieces = gathered_once(running, axis)
        inside, running = (start, start)
        for k in range(length):
            passed = k < here
            running = combine(running, jax.tree.map(lambda part: part[k], pieces))
            inside = jax.tree.map(lambda new, old: jnp.where(passed, new, old), running, inside)
        before = combine(inside, before)
    return before


def split_up(x, dim, length):
    shape = x.shape
    tiles = x.reshape(*shape[:dim], length, shape[dim] // length, *shape[dim + 1 :])
    return jnp.moveaxis(tiles, dim, 0)


def summed_on_arrival(x, axis, dim):
    length = lax.axis_size(axis)
    tiles = lax.all_to_all(split_up(x, dim, length), axis, 0, 0, tiled=True)
    return jnp.sum(tiles.astype(jnp.float32), axis=0)


def joined_along(tiles, dim):
    shape = list(tiles.shape[1:])
    shape[dim] *= tiles.shape[0]
    return jnp.moveaxis(tiles, 0, dim).reshape(shape)


def from_everyone(x, axis):
    copies = jnp.broadcast_to(x, (lax.axis_size(axis), *x.shape))
    return lax.all_to_all(copies, axis, split_axis=0, concat_axis=0, tiled=True)


def gather_directly(x, axis, dim):
    return joined_along(from_everyone(x, axis), dim)


def sent_together(arrays, axis, dim, along):
    both = jnp.concatenate(arrays, axis=along)
    out, at, done = (lax.all_gather(both, axis, axis=dim, tiled=True), 0, [])
    for a in arrays:
        done.append(lax.slice_in_dim(out, at, at + a.shape[along], axis=along))
        at += a.shape[along]
    return tuple(done)


def gather_axes(x, axes, dim):
    for axis in reversed(axes):
        x = lax.all_gather(x, axis, axis=dim, tiled=True)
    return x


def compose(earlier, latter):
    product = jnp.einsum("...ij,...jk->...ik", earlier[0], latter[0], precision=EXACT)
    carried = jnp.einsum("...ij,...jk->...ik", earlier[1], latter[0], precision=EXACT) + latter[1]
    return (product, carried)


def final_output(
    layer_result,
    receptance_rows,
    keys_single,
    values_single,
    self_token_weight,
    head_norm_gain,
    output_gate_preact,
):
    centre = jnp.mean(layer_result, axis=-1, keepdims=True)
    spread = jnp.mean(jnp.square(layer_result - centre), axis=-1, keepdims=True)
    scaled_rows = (layer_result - centre) * lax.rsqrt(spread + GROUP_EPS)
    self_token_term = (
        jnp.sum(receptance_rows * keys_single * self_token_weight[None], axis=-1, keepdims=True)
        * values_single
    )
    sequence_length = layer_result.shape[0]
    heads_merged = scaled_rows.reshape(sequence_length, -1) * head_norm_gain[
        None
    ] + self_token_term.reshape(sequence_length, -1)
    return (heads_merged * jax.nn.sigmoid(output_gate_preact.astype(jnp.float32))).astype(
        jnp.bfloat16
    )


def rms_scale(row_block, gain_vec):
    widened = row_block.astype(jnp.float32)
    factor = lax.rsqrt(jnp.mean(widened * widened, axis=-1, keepdims=True) + NORM_EPS)
    return (widened * factor * gain_vec[None]).astype(jnp.bfloat16)


def per_device(
    receptance,
    head_keys,
    head_values,
    decay_preact,
    learning_rate_preact,
    output_gate_preact,
    self_token_weight,
    head_norm_gain,
    output_weight,
    residual,
    premixer_norm_gain,
    mixer_gate_weight,
    mixer_up_weight,
    mixer_down_weight,
):
    sequence_length = receptance.shape[0]
    head_count = receptance.shape[1] // HEAD_SIZE
    blocks = sequence_length // SUB
    layout = (sequence_length, head_count, HEAD_SIZE)
    receptance_rows = receptance.astype(jnp.float32).reshape(layout)
    keys_single = head_keys.astype(jnp.float32).reshape(layout)
    values_single = head_values.astype(jnp.float32).reshape(layout)
    decay_rate = jnp.exp(-jnp.exp(-jax.nn.softplus(-decay_preact) - 0.5)).reshape(layout)
    learn_rate = jax.nn.sigmoid(learning_rate_preact).reshape(layout)
    unit_key = keys_single / jnp.maximum(jnp.linalg.norm(keys_single, axis=-1, keepdims=True), 1.0)
    remove_dir = -unit_key
    insert_dir = unit_key * learn_rate

    def split_time(values_in):
        return jnp.swapaxes(values_in.reshape(blocks, SUB, head_count, HEAD_SIZE), 0, 1)

    series = tuple(
        (
            split_time(member)
            for member in (
                decay_rate,
                keys_single,
                values_single,
                remove_dir,
                insert_dir,
                receptance_rows,
            )
        )
    )
    head_eye = jnp.broadcast_to(
        jnp.eye(HEAD_SIZE, dtype=jnp.float32), (head_count, HEAD_SIZE, HEAD_SIZE)
    )
    block_eye = jnp.broadcast_to(head_eye[None], (blocks, head_count, HEAD_SIZE, HEAD_SIZE))

    def advance(current, inputs):
        product, memory = current
        decay_t, key_t, value_t, remove_t, insert_t, recept_t = inputs
        shifted = jnp.einsum("bhij,bhj->bhi", product, remove_t, precision=EXACT)
        product = product * decay_t[:, :, None, :] + shifted[..., None] * insert_t[:, :, None, :]
        erased = jnp.einsum("bhij,bhj->bhi", memory, remove_t, precision=EXACT)
        memory = (
            memory * decay_t[:, :, None, :]
            + erased[..., None] * insert_t[:, :, None, :]
            + value_t[..., None] * key_t[:, :, None, :]
        )
        seen_part = jnp.einsum("bhij,bhj->bhi", product, recept_t, precision=EXACT)
        local_part = jnp.einsum("bhij,bhj->bhi", memory, recept_t, precision=EXACT)
        return ((product, memory), (seen_part, local_part))

    (block_prod, block_state), (seen_part, local_part) = lax.scan(
        advance, (block_eye, jnp.zeros_like(block_eye)), series
    )
    inclusive = lax.associative_scan(compose, (block_prod, block_state), axis=0)
    before_prod = jnp.concatenate([head_eye[None], inclusive[0][:-1]], axis=0)
    before_state = jnp.concatenate([jnp.zeros_like(head_eye)[None], inclusive[1][:-1]], axis=0)
    totals = (inclusive[0][-1], inclusive[1][-1])
    incoming = entering(totals, SP, compose, (head_eye, jnp.zeros_like(head_eye)))[1]
    entry_state = (
        jnp.einsum("hij,bhjk->bhik", incoming, before_prod, precision=EXACT) + before_state
    )
    joined = jnp.einsum("bhij,tbhj->tbhi", entry_state, seen_part, precision=EXACT) + local_part
    recurrence_output = jnp.swapaxes(joined, 0, 1).reshape(layout)
    mixer_output = final_output(
        recurrence_output,
        receptance_rows,
        keys_single,
        values_single,
        self_token_weight,
        head_norm_gain,
        output_gate_preact,
    )
    own_rows = sequence_length // lax.axis_size("tp")
    row_start = lax.axis_index("tp") * own_rows
    mix_sum = summed_on_arrival(
        jnp.dot(mixer_output, output_weight, preferred_element_type=jnp.float32).astype(
            jnp.bfloat16
        ),
        "tp",
        0,
    )
    mix = lax.optimization_barrier(mix_sum.astype(jnp.bfloat16)).astype(jnp.float32)
    resid_rows = lax.dynamic_slice_in_dim(residual, row_start, own_rows, 0)
    after_mix = (resid_rows.astype(jnp.float32) + mix).astype(jnp.bfloat16)
    normed = gather_directly(rms_scale(after_mix, premixer_norm_gain), "tp", 0)
    pieces = sent_together((mixer_gate_weight, mixer_up_weight), SP, 0, 1)
    gate_more = jnp.dot(normed, pieces[0], preferred_element_type=jnp.float32)
    up_more = jnp.dot(normed, pieces[1], preferred_element_type=jnp.float32)
    hidden = (jax.nn.silu(gate_more) * up_more).astype(jnp.bfloat16)
    down_full = gather_axes(mixer_down_weight, SP, 1)
    down_sum = summed_on_arrival(
        jnp.dot(hidden, down_full, preferred_element_type=jnp.float32).astype(jnp.bfloat16), "tp", 0
    )
    return (after_mix.astype(jnp.float32) + down_sum).astype(jnp.bfloat16)


def solution(mesh):
    torus = Mesh(mesh.devices.reshape(16, 4, mesh.shape["tp"]), ("sp_0", "sp_1", "tp"))
    in_specs = (
        P(SP, "tp"),
        P(SP, "tp"),
        P(SP, "tp"),
        P(SP, "tp"),
        P(SP, "tp"),
        P(SP, "tp"),
        P("tp", None),
        P("tp"),
        P("tp", None),
        P(SP, None),
        P(),
        P(SP, "tp"),
        P(SP, "tp"),
        P("tp", SP),
    )
    out_specs = P(SP_TP, None)
    return jax.shard_map(
        per_device, mesh=torus, in_specs=in_specs, out_specs=out_specs, check_vma=False
    )
```

profile of v0, /device:TPU:1, one launch (start us, length us, event | category | flops | bytes accessed | tf_op | source)
XLA Modules:
  0.0 540.6 jit_solution(4914291655720536326)
XLA Ops:
  7.6 1.5 convert_multiply_fusion.3
  12.4 150.7 %while.17 = (s32[]{:T(128)}, f32[12,2,64,64]{3,2,1,0:T(8,128)S(1)}, f32[12,2,64,64]{3,2,1,0:T(8,128)S(1)}, f32[16,12,2,64]{3,0,2,1:T(8,128)}, f32[16,12,2,64]{3,...) while((s32[]{:T(128)}, f32[12,2,64,64]{3,2,1,0:T(8,128)S(1)}, ...), condition=%wide.region_2.3_spmd.clone, body=%wide.region_1.2_spmd.clone.sunk | while | flops 5701635 | bytes 3330204 | solution.py:200
  17.3 1.6 dynamic_update_slice.12
  20.2 1.6 dynamic_update_slice.11
  26.7 1.6 dynamic_update_slice.12
  29.6 1.6 dynamic_update_slice.11
  32.6 1.3 fusion.195
  36.2 1.6 dynamic_update_slice.12
  39.1 1.6 dynamic_update_slice.11
  45.6 1.6 dynamic_update_slice.12
  48.5 1.6 dynamic_update_slice.11
  55.0 1.6 dynamic_update_slice.12
  57.9 1.6 dynamic_update_slice.11
  60.9 1.3 fusion.195
  64.4 1.6 dynamic_update_slice.12
  67.4 1.6 dynamic_update_slice.11
  70.3 1.3 fusion.195
  73.9 1.6 dynamic_update_slice.12
  76.8 1.6 dynamic_update_slice.11
  83.3 1.6 dynamic_update_slice.12
  86.2 1.6 dynamic_update_slice.11
  89.2 1.3 fusion.195
  92.7 1.6 dynamic_update_slice.12
  95.6 1.6 dynamic_update_slice.11
  98.6 1.3 fusion.195
  102.1 1.6 dynamic_update_slice.12
  105.1 1.6 dynamic_update_slice.11
  108.0 1.3 fusion.195
  111.5 1.6 dynamic_update_slice.12
  114.5 1.6 dynamic_update_slice.11
  117.4 1.3 fusion.195
  121.0 1.6 dynamic_update_slice.12
  123.9 1.6 dynamic_update_slice.11
  130.4 1.6 dynamic_update_slice.12
  133.3 1.6 dynamic_update_slice.11
  139.8 1.6 dynamic_update_slice.12
  142.7 1.6 dynamic_update_slice.11
  149.2 1.6 dynamic_update_slice.12
  152.1 1.6 dynamic_update_slice.11
  158.6 1.6 dynamic_update_slice.12
  161.5 1.6 dynamic_update_slice.11
  165.9 1.6 pad.45
  168.7 2.6 pad.48
  171.3 2.6 pad.47
  176.3 4.6 pad.50
  181.7 2.6 pad.42
  184.3 2.7 pad.41
  187.0 4.6 pad.49
  192.8 4.6 pad.104
  199.1 11.2 %all-gather = f32[1024,64]{1,0:T(8,128)S(1)} all-gather(f32[256,64]{1,0:T(8,128)S(1)} %pad_maximum_fusion.6), channel_id=2, replica_groups=mesh['sp_0'=16,'sp_1'=4,'tp'=8] {'sp_1'}, dimensions={0}, use_global_device_ids=true | all-gather | bytes 327680 | tf_op jit(solution)/shard_map/all_gather | solution.py:32
  212.7 1.4 pad_maximum_fusion.8
  214.3 11.2 %all_gather.26 = bf16[640,128]{0,1:T(8,128)(2,1)} all-gather(bf16[640,32]{0,1:T(8,128)(2,1)} %param.29), channel_id=1, replica_groups=mesh['sp_0'=16,'sp_1'=4,'tp'=8] {'sp_1'}, dimensions={1}, use_global_device_ids=true | all-gather | bytes 204800 | tf_op jit(solution)/shard_map/all_gather | solution.py:94
  225.6 4.6 pad.73
  237.3 45.9 %all-gather.10.cloned.1.call-done = f32[4096,64]{1,0:T(8,128)} async-done(((f32[256,64]{1,0:T(8,128)}), f32[4096,64]{1,0:T(8,128)}) %all-gather.10.cloned.1.call-update) | async-done | bytes 1048592 | tf_op jit(solution)/shard_map/all_gather | solution.py:32
  284.4 1.4 fusion.101
  290.5 1.4 fusion.104
  294.3 14.6 %all-to-all-start = ((bf16[8,24,2048]{2,1,0:T(8,128)(2,1)}), bf16[8,24,2048]{2,1,0:T(8,128)(2,1)S(1)}, u32[]{:S(2)}, u32[]{:S(2)}) async-start(bf16[8,24,2048]{2,1,0:T(8,128)(2,1)} %bitcast.71), calls=%async_computation | async-start | bytes 1572864 | tf_op jit(solution)/shard_map/all_to_all | solution.py:64
  308.8 12.2 %all-to-all-done = bf16[8,24,2048]{2,1,0:T(8,128)(2,1)S(1)} async-done(((bf16[8,24,2048]{2,1,0:T(8,128)(2,1)}), bf16[8,24,2048]{2,1,0:T(8,128)(2,1)S(1)}, u32[]{:S(2)}, u32[]{:S(2)}) %all-to-all-start) | async-done | bytes 786464 | tf_op jit(solution)/shard_map/all_to_all | solution.py:64
  322.4 15.5 %all_to_all.15 = bf16[8,24,2048]{2,1,0:T(8,128)(2,1)S(1)} all-to-all(bf16[8,24,2048]{2,1,0:T(8,128)(2,1)S(1)} %broadcast_in_dim.45), channel_id=1, replica_groups=mesh['sp_0'=16,'sp_1'=4,'tp'=8] {'tp'}, dimensions={0} | all-to-all | bytes 1572864 | tf_op jit(solution)/shard_map/all_to_all | solution.py:76
  337.9 94.2 %all-gather.6.cloned.1.call-done = bf16[2048,1280]{1,0:T(8,128)(2,1)} async-done(((bf16[32,1280]{1,0:T(8,128)(2,1)}), bf16[2048,1280]{1,0:T(8,128)(2,1)}) %all-gather.6.cloned.1.call-update) | async-done | bytes 5242896 | tf_op jit(solution)/shard_map/all_gather | solution.py:85
  432.1 2.5 fusion.8
  434.6 68.1 %all-gather.8.cloned.1.call-done = bf16[640,2048]{0,1:T(8,128)(2,1)} async-done(((bf16[640,128]{0,1:T(8,128)(2,1)}), bf16[640,2048]{0,1:T(8,128)(2,1)}) %all-gather.8.cloned.1.call-update) | async-done | bytes 2621456 | tf_op jit(solution)/shard_map/all_gather | solution.py:94
  502.7 4.2 convolution_convert_fusion
  506.9 26.3 %all_to_all.16 = bf16[8,24,2048]{2,1,0:T(8,128)(2,1)S(1)} all-to-all(bf16[8,24,2048]{2,1,0:T(8,128)(2,1)S(1)} %bitcast.263), channel_id=1, replica_groups=mesh['sp_0'=16,'sp_1'=4,'tp'=8] {'tp'}, dimensions={0} | all-to-all | bytes 1572864 | tf_op jit(solution)/shard_map/all_to_all | solution.py:64
  (281 shorter events, 123.2 us)
Async XLA Ops:
  6.5 286.4 %copy-start = (bf16[128,2048]{1,0:T(8,128)(2,1)S(1)}, bf16[128,2048]{1,0:T(8,128)(2,1)}, u32[]{:S(2)}) copy-start(bf16[128,2048]{1,0:T(8,128)(2,1)} %param.24) | copy-start | bytes 1572868
  6.5 5.3 copy-start.18
  6.5 5.6 %copy-start.17 = (bf16[192,128]{1,0:T(8,128)(2,1)S(1)}, bf16[192,128]{1,0:T(8,128)(2,1)}, u32[]{:S(2)}) copy-start(bf16[192,128]{1,0:T(8,128)(2,1)} %param.18) | copy-start | bytes 147460
  6.5 276.6 %all-gather.10.cloned.1.call-start = ((), (), s32[]{:S(2)}) async-start(), calls=%async_computation.5 | async-start | bytes 2228224 | tf_op jit(solution)/shard_map/all_gather | solution.py:32
  164.1 1.8 copy-start.4
  181.3 5.7 %copy-start.5 = (f32[5,2,64,64]{3,2,1,0:T(8,128)S(1)}, f32[5,2,64,64]{3,2,1,0:T(8,128)}, u32[]{:S(2)}) copy-start(f32[5,2,64,64]{3,2,1,0:T(8,128)} %convolution_add_fusion.1) | copy-start | bytes 491524
  184.3 13.9 %copy-start.1 = (f32[12,2,64,64]{3,2,1,0:T(8,128)S(1)}, f32[12,2,64,64]{3,2,1,0:T(8,128)}, u32[]{:S(2)}) copy-start(f32[12,2,64,64]{3,2,1,0:T(8,128)} %pad.50) | copy-start | bytes 1179652
  211.4 14.2 %copy-start.6 = (f32[2,64,64]{2,1,0:T(8,128)}, f32[2,64,64]{2,1,0:T(8,128)S(1)}, u32[]{:S(2)}) copy-start(f32[2,64,64]{2,1,0:T(8,128)S(1)} %fusion.108) | copy-start | bytes 98308
  211.6 14.0 %copy-start.8 = (f32[2,64,64]{2,1,0:T(8,128)}, f32[2,64,64]{2,1,0:T(8,128)S(1)}, u32[]{:S(2)}) copy-start(f32[2,64,64]{2,1,0:T(8,128)S(1)} %convolution_add_fusion.23) | copy-start | bytes 98308
  211.8 13.8 %copy-start.10 = (f32[2,64,64]{2,1,0:T(8,128)}, f32[2,64,64]{2,1,0:T(8,128)S(1)}, u32[]{:S(2)}) copy-start(f32[2,64,64]{2,1,0:T(8,128)S(1)} %convolution_add_fusion.22) | copy-start | bytes 98308
  212.0 13.6 %copy-start.12 = (f32[2,64,64]{2,1,0:T(8,128)}, f32[2,64,64]{2,1,0:T(8,128)S(1)}, u32[]{:S(2)}) copy-start(f32[2,64,64]{2,1,0:T(8,128)S(1)} %convolution_add_fusion.21) | copy-start | bytes 98308
  212.7 219.4 %all-gather.6.cloned.1.call-start = ((), (), s32[]{:S(2)}) async-start(), calls=%async_computation.3 | async-start | bytes 5324800 | tf_op jit(solution)/shard_map/all_gather | solution.py:85
  214.2 288.5 %all-gather.8.cloned.1.call-start = ((), (), s32[]{:S(2)}) async-start(), calls=%async_computation.4 | async-start | bytes 2785280 | tf_op jit(solution)/shard_map/all_gather | solution.py:94
  230.1 2.0 copy-start.2
  233.1 4.0 copy-start.7
  286.0 3.3 copy-start.9
  286.0 3.3 copy-start.11
  286.0 3.3 copy-start.13
  286.4 3.1 copy-start.3
  288.0 2.4 copy-start.15
  288.1 2.4 copy-start.16
  289.5 3.4 copy-start.14
  289.6 3.3 copy-start.19
  289.6 3.3 copy-start.21
  292.6 29.6 %copy-start.20 = (f32[2048]{0:T(1024)S(1)}, f32[2048]{0:T(1024)}, u32[]{:S(2)}) copy-start(f32[2048]{0:T(1024)} %param.26) | copy-start | bytes 24580
  294.3 26.7 %all-to-all-start = ((bf16[8,24,2048]{2,1,0:T(8,128)(2,1)}), bf16[8,24,2048]{2,1,0:T(8,128)(2,1)S(1)}, u32[]{:S(2)}, u32[]{:S(2)}) async-start(bf16[8,24,2048]{2,1,0:T(8,128)(2,1)} %bitcast.71), calls=%async_computation | async-start | bytes 1572864 | tf_op jit(solution)/shard_map/all_to_all | solution.py:64
Sparse Core Ops, SparseCore 0:
  212.8 70.3 all-gather.9
  286.1 145.9 all-gather.5
  434.2 68.4 all-gather.7
where the time goes:
time: 543 us; the launch traced here: 541 us
  waiting for transfers between devices  220 us (41%)
  matrix products  107 us (20%)
  local copies, waits for them, and re-layouts  92.3 us (17%)
  blocking collectives  64.3 us (12%)
  other arithmetic  27.2 us (5%)
  starting transfers between devices  14.7 us (3%)
  between operations  14.1 us (3%)
    all_gather x1, waiting for transfers between devices, sent_together(): out, at, done = (lax.all_gather(both, axis, axis=dim, tiled=True), 0, [])  94.2 us
    all_gather x1, waiting for transfers between devices, gather_axes(): x = lax.all_gather(x, axis, axis=dim, tiled=True)  68.1 us
    dynamic_update_slice x32, local copies, waits for them, and re-layouts, per_device(): lax.scan(advance, (block_eye, jnp.zeros_like(block_eye)), series)  51.1 us
    all_gather x1, waiting for transfers between devices, gathered_once(): both, at, found = (lax.all_gather(jnp.concatenate(lines), axis), 0, {})  45.9 us
    all_to_all x1, blocking collectives, summed_on_arrival(): tiles = lax.all_to_all(split_up(x, dim, length), axis, 0, 0, tiled=True)  26.3 us
    pad x10, local copies, waits for them, and re-layouts, per_device(): inclusive = lax.associative_scan(compose, (block_prod, block_state), axis=0)  21.7 us
    dot_general x16, matrix products, advance(): shifted = jnp.einsum('bhij,bhj->bhi', product, remove_t, precision=EXACT)  21.5 us
    dot_general x16, matrix products, advance(): erased = jnp.einsum('bhij,bhj->bhi', memory, remove_t, precision=EXACT)  21.4 us
  transfers between devices with their start and end apart: 4, of which 4 were waited for; matrix products, arithmetic and copies ran while one was open for 5% of the time, Pallas kernels for 0%

commit v1 on v0

v1 whole, which is shorter than its diff:
```python
import functools

import jax
import jax.numpy as jnp
from jax import lax
from jax.experimental import pallas as pl
from jax.experimental.pallas import tpu as pltpu
from jax.sharding import Mesh
from jax.sharding import PartitionSpec as P

HS = 64
CHUNK = 64
W2 = 2 * HS
GROUP_EPS = 0.00064
NORM_EPS = 1e-06
F32 = jnp.float32
BF = jnp.bfloat16
NN = (((1,), (0,)), ((), ()))
NT = (((1,), (1,)), ((), ()))
SEMS = 160


def dg(a, b, dims=NN):
    return lax.dot_general(a, b, dims, preferred_element_type=F32)


def halves(x):
    hi = x.astype(BF)
    return hi, (x - hi.astype(F32)).astype(BF)


def dot_halves(a, b, dims=NN):
    return dg(a[0], b[0], dims) + (dg(a[0], b[1], dims) + dg(a[1], b[0], dims))


def dot3(a, b, dims=NN):
    return dot_halves(halves(a), halves(b), dims)


def dot2(a, b, dims=NN):
    hi, lo = halves(a)
    return dg(hi, b, dims) + dg(lo, b, dims)


def iota(shape, dim):
    return lax.broadcasted_iota(jnp.int32, shape, dim)


def head_masks():
    lane = iota((1, W2), 1)
    first = (lane < HS).astype(F32)
    return first, 1.0 - first


def stacked(x):
    first, second = head_masks()
    return jnp.concatenate([x * first, x * second], axis=0)


def folded(x):
    half = x.shape[0] // 2
    return x[:half] + x[half:]


def head_ones():
    i, j = iota((W2, W2), 0), iota((W2, W2), 1)
    return ((i < HS) == (j < HS)).astype(BF)


def compose(earlier, later):
    moved = dot3(earlier, stacked(later[:HS]))
    return jnp.concatenate([moved[:HS], moved[HS:] + later[HS:]], axis=0)


def identity_pair():
    i, j = iota((W2, W2), 0), iota((W2, W2), 1)
    return ((i == j) | (i + HS == j)).astype(F32) * (i < HS).astype(F32)


def local_chunk(r, k, v, pre, lr):
    logw = jax.nn.sigmoid(pre) * (-0.6065306597126334)
    i, j = iota((CHUNK, CHUNK), 0), iota((CHUNK, CHUNK), 1)
    tri = (i >= j).astype(BF)
    a1 = logw.astype(BF)
    rest = logw - a1.astype(F32)
    a2, a3 = halves(rest)
    cum = dg(tri, a1) + (dg(tri, a2) + dg(tri, a3))
    last = cum[CHUNK - 1 :, :]
    grown = jnp.exp(-cum)
    decayed = jnp.exp(cum)
    tail = jnp.exp(last - cum)
    norm = jnp.sqrt(dot2(k * k, head_ones()))
    unit = k / jnp.maximum(norm, 1.0)
    ins = unit * jax.nn.sigmoid(lr)
    us = stacked(-jnp.exp(cum - logw) * unit)
    rs = stacked(decayed * r)
    bs = stacked(ins * grown)
    ks = stacked(k * grown)
    bts = halves(stacked(ins * tail))
    kts = stacked(k * tail)
    vs = stacked(v).astype(BF)
    gram = dot3(jnp.concatenate([us, rs], axis=0), jnp.concatenate([bs, ks], axis=0), NT)
    i, j = iota((W2, W2), 0), iota((W2, W2), 1)
    same = (i < HS) == (j < HS)
    strict = same & (i > j)
    incl = same & (i >= j)
    lb = jnp.where(strict, gram[:W2, :W2], 0.0)
    lk = jnp.where(strict, gram[:W2, W2:], 0.0)
    mb = jnp.where(incl, gram[W2:, :W2], 0.0)
    mk = jnp.where(incl, gram[W2:, W2:], 0.0)
    inv = (i == j).astype(F32)
    size = 1
    while size < CHUNK:
        row, col = i // size, j // size
        part = jnp.where((row == col + 1) & (row % 2 == 1), lb, 0.0)
        if size == 1:
            inv = inv + part
        else:
            held = halves(inv)
            inv = inv + dot_halves(halves(dot_halves(held, halves(part))), held)
        size *= 2
    lkv = dot2(lk, vs)
    tuv = dot3(inv, jnp.concatenate([us, lkv], axis=1))
    tuv_halves = halves(tuv)
    turned = dot_halves(halves(tuv.T), bts)
    last_col = jnp.where(i == j, jnp.exp(last), 0.0)
    trans = folded(last_col + turned[:W2])
    kth, ktl = halves(kts)
    vt = stacked(v).T.astype(BF)
    state = folded(turned[W2:] + dg(vt, kth) + dg(vt, ktl))
    muv = dot_halves(halves(mb), tuv_halves)
    seen = folded(rs + muv[:, :W2])
    local = folded(muv[:, W2:] + dot2(mk, vs))
    return jnp.concatenate([trans, state], axis=0), seen, local


def kernel(
    nz,
    ny,
    ntp,
    r_ref,
    k_ref,
    v_ref,
    pre_ref,
    lr_ref,
    og_ref,
    stw_ref,
    hg_ref,
    ow_in,
    res_in,
    gain_ref,
    gate_in,
    up_in,
    down_in,
    out_ref,
    gu,
    dn,
    ow,
    res,
    py,
    pz,
    entry,
    seen_ref,
    local_ref,
    self_ref,
    mx,
    am,
    normed,
    hid,
    part,
    got,
    lsem,
    ssem,
    rsem,
    bar_unused,
):
    z, y, tp = lax.axis_index("z"), lax.axis_index("y"), lax.axis_index("tp")
    rows = r_ref.shape[0]
    chunks = rows // CHUNK
    own = rows // ntp
    width = res_in.shape[1]
    half_f = gate_in.shape[0]
    ff = gate_in.shape[1]
    half_ring = nz // 2
    nx = ntp // 2
    xx, core = tp // 2, tp % 2

    def zof(step):
        return lax.rem(z + step + nz, nz)

    def yof(step):
        return lax.rem(y + step + ny, ny)

    def tof(step):
        return lax.rem(tp + step + ntp, ntp)

    def sp(zz, yy):
        return zz * ny + yy

    def dev(zz=None, yy=None, tt=None):
        return {"z": z if zz is None else zz, "y": y if yy is None else yy, "tp": tp if tt is None else tt}

    loads = [
        pltpu.make_async_copy(gate_in, gu.at[sp(z, y), 0:half_f], lsem.at[0]),
        pltpu.make_async_copy(up_in, gu.at[sp(z, y), half_f : 2 * half_f], lsem.at[1]),
        pltpu.make_async_copy(down_in, dn.at[sp(z, y)], lsem.at[2]),
        pltpu.make_async_copy(ow_in, ow.at[tp], lsem.at[3]),
        pltpu.make_async_copy(res_in, res, lsem.at[4]),
    ]
    for load in loads:
        load.start()

    barrier = pltpu.get_barrier_semaphore()
    peers = [dev(zz=zof(1)), dev(zz=zof(-1))]
    peers += [dev(yy=yof(d)) for d in range(1, ny)]
    peers += [dev(tt=tof(d)) for d in range(1, ntp)]
    for peer in peers:
        pl.semaphore_signal(barrier, inc=1, device_id=peer, device_id_type=pl.DeviceIdType.MESH)
    pl.semaphore_wait(barrier, len(peers))
    for load in loads:
        load.wait()

    count = [0]
    sent = []

    def channel():
        count[0] += 1
        return count[0] - 1

    def copy(src, dst, ch, device):
        return pltpu.make_async_remote_copy(
            src_ref=src,
            dst_ref=dst,
            send_sem=ssem.at[ch],
            recv_sem=rsem.at[ch],
            device_id=device,
            device_id_type=pl.DeviceIdType.MESH,
        )

    def send(ref, ch, device):
        c = copy(ref, ref, ch, device)
        c.start()
        sent.append(c)

    def arrived(ref, ch, device):
        copy(ref, ref, ch, device).wait_recv()

    class Ring:
        def __init__(self, block):
            self.block = block
            self.ch = [(channel(), channel()) for _ in range(half_ring)]

        def piece(self, s, side):
            return side if s == half_ring else None

        def push(self, s):
            send(self.block(zof(1 - s), self.piece(s, 0)), self.ch[s - 1][0], dev(zz=zof(1)))
            send(self.block(zof(s - 1), self.piece(s, 1)), self.ch[s - 1][1], dev(zz=zof(-1)))

        def pull(self, s):
            arrived(self.block(zof(-s), self.piece(s, 0)), self.ch[s - 1][0], dev(zz=zof(-1)))
            arrived(self.block(zof(s), self.piece(s, 1)), self.ch[s - 1][1], dev(zz=zof(1)))

    class Across:
        def __init__(self, block):
            self.block = block
            self.ch = [channel() for _ in range(4)]

        def push(self):
            send(self.block(y, None), self.ch[0], dev(yy=yof(1)))
            send(self.block(y, None), self.ch[1], dev(yy=yof(-1)))

        def forward(self):
            arrived(self.block(yof(-1), None), self.ch[0], dev(yy=yof(-1)))
            send(self.block(yof(-1), 0), self.ch[2], dev(yy=yof(1)))
            arrived(self.block(yof(1), None), self.ch[1], dev(yy=yof(1)))
            send(self.block(yof(1), 1), self.ch[3], dev(yy=yof(-1)))

        def finish(self):
            arrived(self.block(yof(2), 0), self.ch[2], dev(yy=yof(-1)))
            arrived(self.block(yof(2), 1), self.ch[3], dev(yy=yof(1)))

    def gu_block(zz, yy, piece):
        slot = sp(zz, yy)
        if piece is None:
            return gu.at[slot]
        return gu.at[slot, piece * half_f : (piece + 1) * half_f]

    def dn_group(zz, piece):
        if piece is None:
            return dn.at[pl.ds(zz * ny, ny)]
        return dn.at[pl.ds(zz * ny + piece * (ny // 2), ny // 2)]

    def dn_block(yy, piece):
        slot = sp(z, yy)
        if piece is None:
            return dn.at[slot]
        return dn.at[slot, piece * (half_f // 2) : (piece + 1) * (half_f // 2)]

    def pz_block(zz, piece):
        if piece is None:
            return pz.at[zz]
        return pz.at[zz, piece * HS : (piece + 1) * HS]

    ring_gu = Ring(lambda zz, piece: gu_block(zz, y, piece))
    ring_dn = Ring(dn_group)
    ring_ps = Ring(pz_block)
    order = [0]
    for s in range(1, half_ring):
        order += [-s, s]
    order += [half_ring]
    across = [
        Across(functools.partial(lambda step, yy, piece: gu_block(zof(step), yy, piece), step))
        for step in order
    ]
    across_dn = Across(dn_block)
    done_across = [0]

    def pump_across(n=1):
        for _ in range(n):
            if done_across[0] < len(across):
                across[done_across[0]].forward()
                done_across[0] += 1

    def same_core(d):
        return lax.rem(xx + d + nx, nx) * 2 + core

    partner = xx * 2 + (1 - core)

    def with_core(d, c):
        return lax.rem(xx + d + nx, nx) * 2 + c

    ow_far = [channel() for _ in range(1, nx)]
    ow_near = [channel() for _ in range(nx)]

    ring_gu.push(1)
    across[0].push()
    across_dn.push()
    for d in range(1, nx):
        send(ow.at[tp], ow_far[d - 1], dev(tt=same_core(d)))
    send(ow.at[tp], ow_near[0], dev(tt=partner))

    ones = head_ones()
    pair = None
    for c in range(chunks):
        span = pl.ds(c * CHUNK, CHUNK)
        r, k, v = (ref[span, :].astype(F32) for ref in (r_ref, k_ref, v_ref))
        ps, seen, local = local_chunk(r, k, v, pre_ref[span, :], lr_ref[span, :])
        seen_ref[span, :] = seen
        local_ref[span, :] = local
        self_ref[span, :] = dot2(r * k * stw_ref[...], ones) * v
        pair = ps if pair is None else compose(pair, ps)
        if c < chunks - 1:
            entry[c] = pair
    py[y] = pair
    ch_y = [channel() for _ in range(1, ny)]
    for d in range(1, ny):
        send(py.at[y], ch_y[d - 1], dev(yy=yof(d)))
    across_dn.forward()
    for d in range(1, ny):
        arrived(py.at[yof(-d)], ch_y[d - 1], dev(yy=yof(-d)))
    inside = identity_pair()
    running = py[0]
    for yy in range(1, ny):
        inside = jnp.where(y == yy, running, inside)
        running = compose(running, py[yy])
    pz[z] = running
    ring_ps.push(1)

    trans_left = identity_pair()[:HS]
    state_left = jnp.zeros((HS, W2), F32)
    state_right = jnp.zeros((HS, W2), F32)
    for s in range(1, half_ring + 1):
        ring_gu.pull(s)
        if s < half_ring:
            ring_gu.push(s + 1)
            across[2 * s - 1].push()
            across[2 * s].push()
        else:
            across[2 * s - 1].push()
        ring_ps.pull(s)
        if s < half_ring:
            ring_ps.push(s + 1)
        pump_across()
        left = pz[zof(-s)]
        has_left = z >= s
        moved = dot3(left, stacked(trans_left))
        trans_left = jnp.where(has_left, moved[:HS], trans_left)
        state_left = jnp.where(has_left, state_left + moved[HS:], state_left)
        if s < half_ring:
            right = pz[zof(s)]
            has_right = z + s >= nz
            state_right = jnp.where(
                has_right, dot3(state_right, stacked(right[:HS])) + right[HS:], state_right
            )
    across_dn.finish()
    ring_dn.push(1)
    state = dot3(state_right, stacked(trans_left)) + state_left
    state = dot3(state, stacked(inside[:HS])) + inside[HS:]

    for c in range(chunks):
        span = pl.ds(c * CHUNK, CHUNK)
        at = state
        if c > 0:
            at = dot3(state, stacked(entry[c - 1][:HS])) + entry[c - 1][HS:]
        o = dot3(seen_ref[span, :], stacked(at), NT) + local_ref[span, :]
        centre = dot2(o, ones) * (1.0 / HS)
        shifted = o - centre
        spread = dot2(shifted * shifted, ones) * (1.0 / HS)
        merged = shifted * lax.rsqrt(spread + GROUP_EPS) * hg_ref[...] + self_ref[span, :]
        gated = merged * jax.nn.sigmoid(og_ref[span, :].astype(F32))
        mx[tp, span, :] = gated.astype(BF)
    ch_mx = [channel() for _ in range(1, ntp)]
    for d in range(1, ntp):
        send(mx.at[tp], ch_mx[d - 1], dev(tt=tof(d)))

    dn_step = [1]

    def pump_dn(n=1):
        for _ in range(n):
            if dn_step[0] <= half_ring:
                ring_dn.pull(dn_step[0])
                if dn_step[0] < half_ring:
                    ring_dn.push(dn_step[0] + 1)
                dn_step[0] += 1

    for d in range(1, nx):
        slot = ow.at[same_core(-d)]
        arrived(slot, ow_far[d - 1], dev(tt=same_core(-d)))
        send(slot, ow_near[d], dev(tt=partner))
    for d in range(1, ntp):
        arrived(mx.at[tof(-d)], ch_mx[d - 1], dev(tt=tof(-d)))
    arrived(ow.at[partner], ow_near[0], dev(tt=partner))
    for d in range(1, nx):
        arrived(ow.at[with_core(-d, 1 - core)], ow_near[d], dev(tt=partner))
    pump_across()
    pump_dn()

    tile = min(256, width)
    tiles = width // tile
    lhs = jnp.concatenate([mx[g] for g in range(ntp)], axis=1)

    def project(n, square):
        cols = pl.ds(pl.multiple_of(n * tile, tile), tile)
        mix = dg(lhs, ow[:, :, cols].reshape(ntp * W2, tile)).astype(BF).astype(F32)
        after = (res[:, cols].astype(F32) + mix).astype(BF).astype(F32)
        am[:, cols] = after
        sq = after * after
        for q in range(tile // W2):
            square = square + sq[:, q * W2 : (q + 1) * W2]
        return square

    square = jnp.zeros((rows, W2), F32)
    square = lax.fori_loop(0, tiles, project, square)
    pump_across()
    pump_dn()
    scale = lax.rsqrt(jnp.sum(square, axis=1, keepdims=True) * (1.0 / width) + NORM_EPS)

    def normalize(n, carry):
        cols = pl.ds(pl.multiple_of(n * tile, tile), tile)
        normed[:, cols] = (am[:, cols] * scale * gain_ref[:, cols]).astype(BF)
        return carry

    lax.fori_loop(0, tiles, normalize, 0)
    while done_across[0] < len(across):
        pump_across()
        pump_dn()
    for a in across:
        a.finish()

    at = 0
    while at < ff:
        wide = min(256, ff - at)
        x = normed[...]
        gate = dg(x, gu[:, 0:half_f, at : at + wide].reshape(width, wide))
        up = dg(x, gu[:, half_f : 2 * half_f, at : at + wide].reshape(width, wide))
        hid[:, at : at + wide] = (gate / (1.0 + jnp.exp(-gate)) * up).astype(BF)
        at += wide
        pump_dn()
    pump_dn(half_ring)

    slots = tile // half_f
    ch_part = [[channel() for _ in range(1, ntp)] for _ in range(2)]

    def down(n, carry):
        cols = pl.ds(pl.multiple_of(n * tile, tile), tile)
        w = dn[pl.ds(n * slots, slots)].reshape(tile, ff)
        prod = dg(hid[...], w, NT)
        part[:, :, cols] = prod.reshape(ntp, own, tile).astype(BF)
        return carry

    half_w = width // 2
    for piece in range(2):
        lax.fori_loop(piece * tiles // 2, (piece + 1) * tiles // 2, down, 0)
        cols = pl.ds(piece * half_w, half_w)
        for d in range(1, ntp):
            c = copy(
                part.at[tof(d), :, cols], got.at[tp, :, cols], ch_part[piece][d - 1], dev(tt=tof(d))
            )
            c.start()
            sent.append(c)
    total = part[tp].astype(F32)
    for d in range(1, ntp):
        for piece in range(2):
            cols = pl.ds(piece * half_w, half_w)
            arrived(got.at[tof(-d), :, cols], ch_part[piece][d - 1], dev(tt=tof(-d)))
        total = total + got[tof(-d)].astype(F32)
    mine = am[pl.ds(pl.multiple_of(tp * own, own), own), :]
    out_ref[...] = (mine + total).astype(BF)
    for c in sent:
        c.wait_send()
    assert count[0] <= SEMS, count[0]


def per_device(
    nz,
    ny,
    ntp,
    receptance,
    head_keys,
    head_values,
    decay_preact,
    learning_rate_preact,
    output_gate_preact,
    self_token_weight,
    head_norm_gain,
    output_weight,
    residual,
    premixer_norm_gain,
    mixer_gate_weight,
    mixer_up_weight,
    mixer_down_weight,
):
    rows = receptance.shape[0]
    width = residual.shape[1]
    half_f, ff = mixer_gate_weight.shape
    own = rows // ntp
    vmem = pl.BlockSpec(memory_space=pltpu.VMEM)
    hbm = pl.BlockSpec(memory_space=pl.ANY)
    return pl.pallas_call(
        functools.partial(kernel, nz, ny, ntp),
        out_shape=jax.ShapeDtypeStruct((own, width), BF),
        in_specs=[vmem] * 8 + [hbm, hbm, vmem, hbm, hbm, hbm],
        out_specs=vmem,
        scratch_shapes=[
            pltpu.VMEM((nz * ny, 2 * half_f, ff), BF),
            pltpu.VMEM((nz * ny, half_f, ff), BF),
            pltpu.VMEM((ntp, W2, width), BF),
            pltpu.VMEM((rows, width), BF),
            pltpu.VMEM((ny, W2, W2), F32),
            pltpu.VMEM((nz, W2, W2), F32),
            pltpu.VMEM((rows // CHUNK, W2, W2), F32),
            pltpu.VMEM((rows, W2), F32),
            pltpu.VMEM((rows, W2), F32),
            pltpu.VMEM((rows, W2), F32),
            pltpu.VMEM((ntp, rows, W2), BF),
            pltpu.VMEM((rows, width), F32),
            pltpu.VMEM((rows, width), BF),
            pltpu.VMEM((rows, ff), BF),
            pltpu.VMEM((ntp, own, width), BF),
            pltpu.VMEM((ntp, own, width), BF),
            pltpu.SemaphoreType.DMA((5,)),
            pltpu.SemaphoreType.DMA((SEMS,)),
            pltpu.SemaphoreType.DMA((SEMS,)),
            pltpu.SMEM((1,), jnp.int32),
        ],
        compiler_params=pltpu.CompilerParams(
            collective_id=0, has_side_effects=True, vmem_limit_bytes=60 * 1024 * 1024
        ),
        name="layer",
    )(
        receptance,
        head_keys,
        head_values,
        decay_preact,
        learning_rate_preact,
        output_gate_preact,
        self_token_weight.reshape(1, -1),
        head_norm_gain.reshape(1, -1),
        output_weight,
        residual,
        premixer_norm_gain.reshape(1, -1),
        mixer_gate_weight,
        mixer_up_weight,
        mixer_down_weight.T,
    )


def build(mesh, nz, ny):
    ntp = mesh.shape["tp"]
    torus = Mesh(mesh.devices.reshape(nz, ny, ntp), ("z", "y", "tp"))
    sp = ("z", "y")
    cut = P(sp, "tp")
    in_specs = (cut,) * 6 + (
        P("tp", None),
        P("tp"),
        P("tp", None),
        P(sp, None),
        P(),
        cut,
        cut,
        P("tp", sp),
    )
    return jax.shard_map(
        functools.partial(per_device, nz, ny, ntp),
        mesh=torus,
        in_specs=in_specs,
        out_specs=P(("z", "y", "tp"), None),
        check_vma=False,
    )


def solution(mesh):
    return build(mesh, 16, 4)
```

time: 543 us -> 122 us (0.22)
  waiting for transfers between devices: 220 us -> 0 us
  Pallas kernels: 0 us -> 119 us
  matrix products: 107 us -> 0 us
  local copies, waits for them, and re-layouts: 92.3 us -> 2.81 us
  blocking collectives: 64.3 us -> 0 us
  other arithmetic: 27.2 us -> 0 us
  starting transfers between devices: 14.7 us -> 0 us
  between operations: 14.1 us -> 0.01 us
    all_gather x3 -> x0, waiting for transfers between devices: 208 us -> none  [the longest x1 94.2 us: sent_together(): out, at, done = (lax.all_gather(both, axis, axis=dim, tiled=True), 0, [])]
    pallas_call x0 -> x1, Pallas kernels: none -> 119 us  [per_device(): pl.pallas_call(functools.partial(kernel, nz, ny, ntp), out_shape=jax.Shap...]
    dot_general x108 -> x0, matrix products: 107 us -> none  [the longest x16 21.5 us: advance(): shifted = jnp.einsum('bhij,bhj->bhi', product, remove_t, precision=EXACT)]
    dynamic_update_slice x32 -> x0, local copies, waits for them, and re-layouts: 51.1 us -> none  [per_device(): lax.scan(advance, (block_eye, jnp.zeros_like(block_eye)), series)]
    all_to_all x2 -> x0, blocking collectives: 41.9 us -> none  [the longest x1 26.3 us: summed_on_arrival(): tiles = lax.all_to_all(split_up(x, dim, length), axis, 0, 0, tiled=True)]
    all_gather x2 -> x0, blocking collectives: 22.5 us -> none  [the longest x1 11.2 us: gathered_once(): both, at, found = (lax.all_gather(jnp.concatenate(lines), axis), 0, {})]
    pad x10 -> x0, local copies, waits for them, and re-layouts: 21.7 us -> none  [per_device(): inclusive = lax.associative_scan(compose, (block_prod, block_state), axis=0)]
    add x23 -> x0, other arithmetic: 17.1 us -> none  [the longest x16 12.9 us: advance(): memory * decay_t[:, :, None, :]]
  transfers between devices with their start and end apart: 4 -> 0, of which waited for: 4 -> 0; matrix products, arithmetic and copies ran while one was open for 5% -> 0% of each run, Pallas kernels for 0% -> 0%
where the time goes in v1:
time: 122 us
  Pallas kernels  119 us (98%)
  local copies, waits for them, and re-layouts  2.81 us (2%)
    pallas_call x1, Pallas kernels, per_device(): pl.pallas_call(functools.partial(kernel, nz, ny, ntp), out_shape=jax.Shap...  119 us

profile of v1, /device:TPU:1, one launch (start us, length us, event | category | flops | bytes accessed | tf_op | source)
XLA Modules:
  0.0 122.3 jit_solution(14268674164183712516)
XLA Ops:
  0.0 0.0 copy-start
  0.0 0.7 copy-done
  0.7 0.6 reshape.9.stw_ref
  1.3 119.5 %layer.1 = bf16[24,2048]{1,0:T(8,128)(2,1)} custom-call(bf16[192,128]{1,0:T(8,128)(2,1)} %r_ref.1, bf16[192,128]{1,0:T(8,128)(2,1)} %k_ref.1, bf16[192,128]{1,0:T(8,128)(2,1)} %v_ref.1, f32[192,128]{1,0:T(8,128)} %pre_ref.1, f32[192,128]{1,0:T(8,128)} %lr_ref.1, bf16[192,128]{1,0:T(8,128)(2,1)} %og_ref.1, f32[1,128]{1,0:T(1,128)} %reshape.9.stw_ref, ...), custom_call_target="tpu_custom_call" | custom-call | tf_op jit(solution)/shard_map/layer/pallas_call | solution.py:540
  120.8 1.5 %copy.16 = bf16[24,2048]{1,0:T(8,128)(2,1)} copy(bf16[24,2048]{1,0:T(8,128)(2,1)} %layer.1) | data formatting | bytes 196608
Async XLA Ops:
  0.0 0.7 copy-start

commit v2 on v1

v2 whole, which is shorter than its diff:
```python
import functools

import jax
import jax.numpy as jnp
from jax import lax
from jax.experimental import pallas as pl
from jax.experimental.pallas import tpu as pltpu
from jax.sharding import Mesh
from jax.sharding import PartitionSpec as P

HS = 64
CHUNK = 64
W2 = 2 * HS
GROUP_EPS = 0.00064
NORM_EPS = 1e-06
F32 = jnp.float32
BF = jnp.bfloat16
NN = (((1,), (0,)), ((), ()))
NT = (((1,), (1,)), ((), ()))
SEMS = 200


def dg(a, b, dims=NN):
    return lax.dot_general(a, b, dims, preferred_element_type=F32)


def halves(x):
    hi = x.astype(BF)
    return hi, (x - hi.astype(F32)).astype(BF)


def dot_halves(a, b, dims=NN):
    return dg(a[0], b[0], dims) + (dg(a[0], b[1], dims) + dg(a[1], b[0], dims))


def dot3(a, b, dims=NN):
    return dot_halves(halves(a), halves(b), dims)


def dot2(a, b, dims=NN):
    hi, lo = halves(a)
    return dg(hi, b, dims) + dg(lo, b, dims)


def iota(shape, dim):
    return lax.broadcasted_iota(jnp.int32, shape, dim)


def head_masks():
    lane = iota((1, W2), 1)
    first = (lane < HS).astype(F32)
    return first, 1.0 - first


def stacked(x):
    first, second = head_masks()
    return jnp.concatenate([x * first, x * second], axis=0)


def folded(x):
    half = x.shape[0] // 2
    return x[:half] + x[half:]


def head_ones():
    i, j = iota((W2, W2), 0), iota((W2, W2), 1)
    return ((i < HS) == (j < HS)).astype(BF)


def compose(earlier, later):
    moved = dot3(earlier, stacked(later[:HS]))
    return jnp.concatenate([moved[:HS], moved[HS:] + later[HS:]], axis=0)


def identity_pair():
    i, j = iota((W2, W2), 0), iota((W2, W2), 1)
    return ((i == j) | (i + HS == j)).astype(F32) * (i < HS).astype(F32)


def chunk_stages(chunks):
    i, j = iota((CHUNK, CHUNK), 0), iota((CHUNK, CHUNK), 1)
    tri = (i >= j).astype(BF)
    ones = head_ones()
    i, j = iota((W2, W2), 0), iota((W2, W2), 1)
    same = (i < HS) == (j < HS)
    strict = same & (i > j)
    incl = same & (i >= j)
    made = []
    for r, k, v, pre, lr in chunks:
        logw = jax.nn.sigmoid(pre) * (-0.6065306597126334)
        a1 = logw.astype(BF)
        a2, a3 = halves(logw - a1.astype(F32))
        cum = dg(tri, a1) + (dg(tri, a2) + dg(tri, a3))
        last = cum[CHUNK - 1 :, :]
        grown = jnp.exp(-cum)
        tail = jnp.exp(last - cum)
        unit = k / jnp.maximum(jnp.sqrt(dot2(k * k, ones)), 1.0)
        ins = unit * jax.nn.sigmoid(lr)
        us = stacked(-jnp.exp(cum - logw) * unit)
        rs = stacked(jnp.exp(cum) * r)
        made.append(
            dict(
                last=last,
                us=us,
                rs=rs,
                left=halves(jnp.concatenate([us, rs], axis=0)),
                right=halves(
                    jnp.concatenate([stacked(ins * grown), stacked(k * grown)], axis=0)
                ),
                bts=halves(stacked(ins * tail)),
                kts=halves(stacked(k * tail)),
                v=stacked(v),
            )
        )
    yield
    for m in made:
        gram = dot_halves(m["left"], m["right"], NT)
        m["lb"] = jnp.where(strict, gram[:W2, :W2], 0.0)
        m["lk"] = jnp.where(strict, gram[:W2, W2:], 0.0)
        m["mb"] = jnp.where(incl, gram[W2:, :W2], 0.0)
        m["mk"] = jnp.where(incl, gram[W2:, W2:], 0.0)
        m["vs"] = m["v"].astype(BF)
    for m in made:
        m["lkv"] = dot2(m["lk"], m["vs"])
        m["mkv"] = dot2(m["mk"], m["vs"])
    yield
    size = 1
    while size < CHUNK:
        row, col = i // size, j // size
        below = (row == col + 1) & (row % 2 == 1)
        if size == 1:
            for m in made:
                m["inv"] = (i == j).astype(F32) + jnp.where(below, m["lb"], 0.0)
        else:
            held = [halves(m["inv"]) for m in made]
            mid = [
                dot_halves(h, halves(jnp.where(below, m["lb"], 0.0))) for h, m in zip(held, made)
            ]
            for m, h, x in zip(made, held, mid):
                m["inv"] = m["inv"] + dot_halves(halves(x), h)
        size *= 2
        if size == 8 or size == 32:
            yield
    for m in made:
        m["tuv"] = dot3(m["inv"], jnp.concatenate([m["us"], m["lkv"]], axis=1))
    out = []
    for m in made:
        turned = dot_halves(halves(m["tuv"].T), m["bts"])
        trans = folded(jnp.where(i == j, jnp.exp(m["last"]), 0.0) + turned[:W2])
        vt = m["v"].T.astype(BF)
        state = folded(turned[W2:] + dg(vt, m["kts"][0]) + dg(vt, m["kts"][1]))
        m["pair"] = jnp.concatenate([trans, state], axis=0)
    for m in made:
        muv = dot_halves(halves(m["mb"]), halves(m["tuv"]))
        out.append(
            (m["pair"], folded(m["rs"] + muv[:, :W2]), folded(muv[:, W2:] + m["mkv"]))
        )
    return out


def kernel(
    nz,
    ny,
    ntp,
    r_ref,
    k_ref,
    v_ref,
    pre_ref,
    lr_ref,
    og_ref,
    stw_ref,
    hg_ref,
    ow_in,
    res_in,
    gain_ref,
    gate_in,
    up_in,
    down_in,
    out_ref,
    gu,
    dn,
    ow,
    res,
    py,
    pz,
    entry,
    seen_ref,
    local_ref,
    self_ref,
    mx,
    am,
    normed,
    hid,
    part,
    got,
    pgot,
    comb,
    lsem,
    ssem,
    rsem,
):
    z, y, tp = lax.axis_index("z"), lax.axis_index("y"), lax.axis_index("tp")
    rows = r_ref.shape[0]
    chunks = rows // CHUNK
    own = rows // ntp
    width = res_in.shape[1]
    half_f = gate_in.shape[0]
    ff = gate_in.shape[1]
    half_ring = nz // 2
    nx = ntp // 2
    xx, core = tp // 2, tp % 2

    def zof(step):
        return lax.rem(z + step + nz, nz)

    def yof(step):
        return lax.rem(y + step + ny, ny)

    def tof(step):
        return lax.rem(tp + step + ntp, ntp)

    def sp(zz, yy):
        return zz * ny + yy

    def dev(zz=None, yy=None, tt=None):
        return {"z": z if zz is None else zz, "y": y if yy is None else yy, "tp": tp if tt is None else tt}

    scope = [None]

    def mark(name):
        if scope[0] is not None:
            scope[0].__exit__(None, None, None)
        scope[0] = None
        if name:
            scope[0] = jax.named_scope(name)
            scope[0].__enter__()

    mark("enter")
    loads = [
        pltpu.make_async_copy(gate_in, gu.at[sp(z, y), 0:half_f], lsem.at[0]),
        pltpu.make_async_copy(up_in, gu.at[sp(z, y), half_f : 2 * half_f], lsem.at[1]),
        pltpu.make_async_copy(down_in, dn.at[sp(z, y)], lsem.at[2]),
        pltpu.make_async_copy(ow_in, ow.at[tp], lsem.at[3]),
        pltpu.make_async_copy(res_in, res, lsem.at[4]),
    ]
    for load in loads:
        load.start()

    barrier = pltpu.get_barrier_semaphore()
    peers = [dev(zz=zof(1)), dev(zz=zof(-1))]
    peers += [dev(yy=yof(d)) for d in range(1, ny)]
    peers += [dev(tt=tof(d)) for d in range(1, ntp)]
    for peer in peers:
        pl.semaphore_signal(barrier, inc=1, device_id=peer, device_id_type=pl.DeviceIdType.MESH)
    pl.semaphore_wait(barrier, len(peers))
    for load in loads:
        load.wait()

    count = [0]
    sent = []

    def channel():
        count[0] += 1
        return count[0] - 1

    def copy(src, dst, ch, device):
        return pltpu.make_async_remote_copy(
            src_ref=src,
            dst_ref=dst,
            send_sem=ssem.at[ch],
            recv_sem=rsem.at[ch],
            device_id=device,
            device_id_type=pl.DeviceIdType.MESH,
        )

    def send(ref, ch, device):
        c = copy(ref, ref, ch, device)
        c.start()
        sent.append(c)

    def arrived(ref, ch, device):
        copy(ref, ref, ch, device).wait_recv()

    class Ring:
        def __init__(self, block):
            self.block = block
            self.ch = [(channel(), channel()) for _ in range(half_ring)]
            self.step = 1

        def piece(self, s, side):
            return side if s == half_ring else None

        def push(self, s):
            send(self.block(zof(1 - s), self.piece(s, 0)), self.ch[s - 1][0], dev(zz=zof(1)))
            send(self.block(zof(s - 1), self.piece(s, 1)), self.ch[s - 1][1], dev(zz=zof(-1)))

        def turn(self):
            s = self.step
            if s > half_ring:
                return
            arrived(self.block(zof(-s), self.piece(s, 0)), self.ch[s - 1][0], dev(zz=zof(-1)))
            arrived(self.block(zof(s), self.piece(s, 1)), self.ch[s - 1][1], dev(zz=zof(1)))
            if s < half_ring:
                self.push(s + 1)
            self.step = s + 1

    class Across:
        def __init__(self, block, at, to):
            self.block, self.at, self.to = block, at, to
            self.ch = [channel() for _ in range(4)]

        def push(self):
            send(self.block(self.at(0), None), self.ch[0], self.to(1))
            send(self.block(self.at(0), None), self.ch[1], self.to(-1))

        def forward(self):
            arrived(self.block(self.at(-1), None), self.ch[0], self.to(-1))
            send(self.block(self.at(-1), 0), self.ch[2], self.to(1))
            arrived(self.block(self.at(1), None), self.ch[1], self.to(1))
            send(self.block(self.at(1), 1), self.ch[3], self.to(-1))

        def finish(self):
            arrived(self.block(self.at(2), 0), self.ch[2], self.to(-1))
            arrived(self.block(self.at(2), 1), self.ch[3], self.to(1))

    def cut(ref, piece, size):
        return ref if piece is None else ref.at[piece * size : (piece + 1) * size]

    def gu_block(zz, yy, piece):
        return cut(gu.at[sp(zz, yy)], piece, half_f)

    def dn_pair(which, zz, piece):
        if piece is None:
            return dn.at[pl.ds(zz * ny + which * (ny // 2), ny // 2)]
        return dn.at[pl.ds(zz * ny + which * (ny // 2) + piece * (ny // 4), ny // 4)]

    def y_dev(d):
        return dev(yy=yof(d))

    ring_gu = Ring(lambda zz, piece: gu_block(zz, y, piece))
    ring_d0 = Ring(functools.partial(dn_pair, 0))
    ring_d1 = Ring(functools.partial(dn_pair, 1))
    ring_ps = Ring(lambda zz, piece: cut(pz.at[zz], piece, HS))
    order = [0]
    for s in range(1, half_ring):
        order += [-s, s]
    order += [half_ring]
    across = [
        Across(
            functools.partial(lambda step, yy, piece: gu_block(zof(step), yy, piece), step),
            yof,
            y_dev,
        )
        for step in order
    ]
    across_dn = Across(lambda yy, piece: cut(dn.at[sp(z, yy)], piece, half_f // 2), yof, y_dev)

    bulk = [ring_gu] * 3 + [ring_d0]
    while len(bulk) < 3 * half_ring:
        bulk += [ring_d1, ring_gu, ring_d0]
    bulk += [ring_d1] * half_ring + [ring_d0] * half_ring
    progress = {"bulk": 0, "push": 1, "forward": 0}

    def turn(n=1):
        done = 0
        while done < n and progress["bulk"] < len(bulk):
            ring = bulk[progress["bulk"]]
            progress["bulk"] += 1
            if ring.step <= half_ring:
                ring.turn()
                done += 1

    def y_push(n=1):
        for _ in range(n):
            i = progress["push"]
            if i < len(across) and (i + 1) // 2 < ring_gu.step:
                across[i].push()
                progress["push"] += 1

    def y_forward(n=1):
        for _ in range(n):
            if progress["forward"] < progress["push"]:
                across[progress["forward"]].forward()
                progress["forward"] += 1

    def same_core(d):
        return lax.rem(xx + d + nx, nx) * 2 + core

    def other_core(d):
        return lax.rem(xx + d + nx, nx) * 2 + (1 - core)

    def x_dev(d):
        return dev(tt=same_core(d))

    partner = other_core(0)
    near = dev(tt=partner)
    across_ow = None
    if nx == 4:
        across_ow = Across(lambda t, piece: cut(ow.at[t], piece, W2 // 2), same_core, x_dev)
    ow_far = [channel() for _ in range(1, nx)]
    ow_near = [channel() for _ in range(nx)]

    def ow_start():
        if across_ow is not None:
            across_ow.push()
        else:
            for d in range(1, nx):
                send(ow.at[tp], ow_far[d - 1], x_dev(d))
        send(ow.at[tp], ow_near[0], near)

    def ow_share(d):
        send(ow.at[same_core(d)], ow_near[d % nx], near)

    def ow_middle():
        if across_ow is not None:
            across_ow.forward()
            ow_share(1)
            ow_share(-1)

    def ow_last():
        if across_ow is not None:
            across_ow.finish()
            ow_share(2)
        else:
            for d in range(1, nx):
                arrived(ow.at[same_core(-d)], ow_far[d - 1], x_dev(-d))
                ow_share(-d)

    def ow_finish():
        for d in range(nx):
            arrived(ow.at[other_core(d)], ow_near[d], near)

    mark("launch")
    ring_gu.push(1)
    across[0].push()
    across_dn.push()
    ow_start()

    mark("recur")
    ones = head_ones()
    spans = [pl.ds(c * CHUNK, CHUNK) for c in range(chunks)]
    given = []
    for span in spans:
        r, k, v = (ref[span, :].astype(F32) for ref in (r_ref, k_ref, v_ref))
        given.append((r, k, v, pre_ref[span, :], lr_ref[span, :]))
    stages = chunk_stages(given)
    stage = 0
    while True:
        try:
            next(stages)
        except StopIteration as end:
            made = end.value
            break
        mark(f"recur_pump{stage}")
        if stage == 1:
            turn()
            y_push()
        if stage == 2:
            across_dn.forward()
        if stage == 3:
            turn()
            y_forward()
        stage += 1
        mark(f"recur{stage}")
    pair = None
    for c, (ps, seen, local) in enumerate(made):
        seen_ref[spans[c], :] = seen
        local_ref[spans[c], :] = local
        pair = ps if pair is None else compose(pair, ps)
        if c < chunks - 1:
            entry[c] = pair
    mark("scan_y")
    py[y] = pair
    ch_y = [channel() for _ in range(1, ny)]
    for d in range(1, ny):
        send(py.at[y], ch_y[d - 1], dev(yy=yof(d)))
    y_push(2)
    across_dn.finish()
    ring_d0.push(1)
    for c, (r, k, v, _, _) in enumerate(given):
        self_ref[spans[c], :] = dot2(r * k * stw_ref[...], ones) * v
    turn()
    mark("scan_ywait")
    ring_d1.push(1)
    for d in range(1, ny):
        arrived(py.at[yof(-d)], ch_y[d - 1], dev(yy=yof(-d)))
    mark("scan_yfix")
    inside = identity_pair()
    running = py[0]
    for yy in range(1, ny):
        inside = jnp.where(y == yy, running, inside)
        running = compose(running, py[yy])
    pz[z] = running
    ring_ps.push(1)

    trans_left = identity_pair()[:HS]
    state_left = jnp.zeros((HS, W2), F32)
    state_right = jnp.zeros((HS, W2), F32)
    for s in range(1, half_ring + 1):
        mark(f"scan_z{s}")
        turn()
        ring_ps.turn()
        y_push()
        y_forward()
        if s == half_ring // 2:
            ow_middle()
        if s == half_ring - 1:
            ow_last()
        left = pz[zof(-s)]
        has_left = z >= s
        moved = dot3(left, stacked(trans_left))
        trans_left = jnp.where(has_left, moved[:HS], trans_left)
        state_left = jnp.where(has_left, state_left + moved[HS:], state_left)
        if s < half_ring:
            right = pz[zof(s)]
            has_right = z + s >= nz
            state_right = jnp.where(
                has_right, dot3(state_right, stacked(right[:HS])) + right[HS:], state_right
            )
    mark("state")
    state = dot3(state_right, stacked(trans_left)) + state_left
    state = dot3(state, stacked(inside[:HS])) + inside[HS:]

    mark("mech")
    for c in range(chunks):
        span = spans[c]
        at = state
        if c > 0:
            at = dot3(state, stacked(entry[c - 1][:HS])) + entry[c - 1][HS:]
        o = dot3(seen_ref[span, :], stacked(at), NT) + local_ref[span, :]
        centre = dot2(o, ones) * (1.0 / HS)
        shifted = o - centre
        spread = dot2(shifted * shifted, ones) * (1.0 / HS)
        merged = shifted * lax.rsqrt(spread + GROUP_EPS) * hg_ref[...] + self_ref[span, :]
        gated = merged * jax.nn.sigmoid(og_ref[span, :].astype(F32))
        mx[tp, span, :] = gated.astype(BF)
    mx_far = [channel() for _ in range(1, nx)]
    mx_near = [channel() for _ in range(nx)]
    for d in range(1, nx):
        send(mx.at[tp], mx_far[d - 1], x_dev(d))
    send(mx.at[tp], mx_near[0], near)
    mark("exch_pump")
    turn(2)
    y_push()
    y_forward()
    mark("exch_far")
    for d in range(1, nx):
        slot = mx.at[same_core(-d)]
        arrived(slot, mx_far[d - 1], x_dev(-d))
        send(slot, mx_near[d], near)
    mark("exch_near")
    for d in range(nx):
        arrived(mx.at[other_core(-d)], mx_near[d], near)
    mark("exch_ow")
    ow_finish()
    mark("exch_pump2")
    turn(2)
    y_push()
    y_forward()

    mark("project")
    tile = min(256, width)
    tiles = width // tile
    lhs = jnp.concatenate([mx[g] for g in range(ntp)], axis=1)

    def project(n, square):
        cols = pl.ds(pl.multiple_of(n * tile, tile), tile)
        mix = dg(lhs, ow[:, :, cols].reshape(ntp * W2, tile)).astype(BF).astype(F32)
        after = (res[:, cols].astype(F32) + mix).astype(BF).astype(F32)
        am[:, cols] = after
        sq = after * after
        for q in range(tile // W2):
            square = square + sq[:, q * W2 : (q + 1) * W2]
        return square

    square = jnp.zeros((rows, W2), F32)
    square = lax.fori_loop(0, tiles, project, square)
    mark("norm")
    scale = lax.rsqrt(jnp.sum(square, axis=1, keepdims=True) * (1.0 / width) + NORM_EPS)

    def normalize(n, carry):
        cols = pl.ds(pl.multiple_of(n * tile, tile), tile)
        normed[:, cols] = (am[:, cols] * scale * gain_ref[:, cols]).astype(BF)
        return carry

    lax.fori_loop(0, tiles, normalize, 0)
    mark("pumprest")
    while progress["forward"] < len(across):
        turn()
        y_push(2)
        y_forward()
    mark("finish")
    for a in across:
        a.finish()

    mark("gateup")
    at = 0
    while at < ff:
        wide = min(256, ff - at)
        x = normed[...]
        gate = dg(x, gu[:, 0:half_f, at : at + wide].reshape(width, wide))
        up = dg(x, gu[:, half_f : 2 * half_f, at : at + wide].reshape(width, wide))
        hid[:, at : at + wide] = (gate / (1.0 + jnp.exp(-gate)) * up).astype(BF)
        at += wide
        turn()
    mark("dnwait")
    turn(3 * half_ring)

    slots = tile // half_f
    half_w = width // 2

    def down(n, carry):
        cols = pl.ds(pl.multiple_of(n * tile, tile), tile)
        w = dn[pl.ds(n * slots, slots)].reshape(tile, ff)
        prod = dg(hid[...], w, NT).reshape(nx, 2, own, tile).astype(BF)
        part[0, :, :, cols] = prod[:, 0]
        part[1, :, :, cols] = prod[:, 1]
        return carry

    def pass_on(src, dst, ch, device):
        c = copy(src, dst, ch, device)
        c.start()
        sent.append(c)

    pieces = [pl.ds(piece * half_w, half_w) for piece in range(2)]
    ch_core = [channel() for _ in range(2)]
    ch_part = [[channel() for _ in range(1, nx)] for _ in range(2)]
    for piece, cols in enumerate(pieces):
        mark(f"down{piece}")
        lax.fori_loop(piece * tiles // 2, (piece + 1) * tiles // 2, down, 0)
        pass_on(part.at[1 - core, :, :, cols], pgot.at[:, :, cols], ch_core[piece], near)

    def x_at(d):
        return lax.rem(xx + d + nx, nx)

    for piece, cols in enumerate(pieces):
        mark(f"rs_core{piece}")
        arrived(pgot.at[:, :, cols], ch_core[piece], near)
        for d in [2, 1, 3] if nx == 4 else range(1, nx):
            both = part[core, x_at(d), :, cols].astype(F32) + pgot[x_at(d), :, cols].astype(F32)
            comb[d - 1, :, cols] = both.astype(BF)
            pass_on(comb.at[d - 1, :, cols], got.at[d - 1, :, cols], ch_part[piece][d - 1], x_dev(d))
    mark("rs_wait")
    for piece, cols in enumerate(pieces):
        total = am[pl.ds(pl.multiple_of(tp * own, own), own), cols]
        total = total + part[core, xx, :, cols].astype(F32) + pgot[xx, :, cols].astype(F32)
        for d in range(1, nx):
            arrived(got.at[d - 1, :, cols], ch_part[piece][d - 1], x_dev(-d))
            total = total + got[d - 1, :, cols].astype(F32)
        out_ref[:, cols] = total.astype(BF)
    mark("sendwait")
    for c in sent:
        c.wait_send()
    mark(None)
    assert count[0] <= SEMS, count[0]


def per_device(
    nz,
    ny,
    ntp,
    receptance,
    head_keys,
    head_values,
    decay_preact,
    learning_rate_preact,
    output_gate_preact,
    self_token_weight,
    head_norm_gain,
    output_weight,
    residual,
    premixer_norm_gain,
    mixer_gate_weight,
    mixer_up_weight,
    mixer_down_weight,
):
    rows = receptance.shape[0]
    width = residual.shape[1]
    half_f, ff = mixer_gate_weight.shape
    own = rows // ntp
    nx = ntp // 2
    vmem = pl.BlockSpec(memory_space=pltpu.VMEM)
    hbm = pl.BlockSpec(memory_space=pl.ANY)
    return pl.pallas_call(
        functools.partial(kernel, nz, ny, ntp),
        out_shape=jax.ShapeDtypeStruct((own, width), BF),
        in_specs=[vmem] * 8 + [hbm, hbm, vmem, hbm, hbm, hbm],
        out_specs=vmem,
        scratch_shapes=[
            pltpu.VMEM((nz * ny, 2 * half_f, ff), BF),
            pltpu.VMEM((nz * ny, half_f, ff), BF),
            pltpu.VMEM((ntp, W2, width), BF),
            pltpu.VMEM((rows, width), BF),
            pltpu.VMEM((ny, W2, W2), F32),
            pltpu.VMEM((nz, W2, W2), F32),
            pltpu.VMEM((rows // CHUNK, W2, W2), F32),
            pltpu.VMEM((rows, W2), F32),
            pltpu.VMEM((rows, W2), F32),
            pltpu.VMEM((rows, W2), F32),
            pltpu.VMEM((ntp, rows, W2), BF),
            pltpu.VMEM((rows, width), F32),
            pltpu.VMEM((rows, width), BF),
            pltpu.VMEM((rows, ff), BF),
            pltpu.VMEM((2, nx, own, width), BF),
            pltpu.VMEM((max(nx - 1, 1), own, width), BF),
            pltpu.VMEM((nx, own, width), BF),
            pltpu.VMEM((max(nx - 1, 1), own, width), BF),
            pltpu.SemaphoreType.DMA((5,)),
            pltpu.SemaphoreType.DMA((SEMS,)),
            pltpu.SemaphoreType.DMA((SEMS,)),
        ],
        compiler_params=pltpu.CompilerParams(
            collective_id=0, has_side_effects=True, vmem_limit_bytes=60 * 1024 * 1024
        ),
        name="layer",
    )(
        receptance,
        head_keys,
        head_values,
        decay_preact,
        learning_rate_preact,
        output_gate_preact,
        self_token_weight.reshape(1, -1),
        head_norm_gain.reshape(1, -1),
        output_weight,
        residual,
        premixer_norm_gain.reshape(1, -1),
        mixer_gate_weight,
        mixer_up_weight,
        mixer_down_weight.T,
    )


def build(mesh, nz, ny):
    ntp = mesh.shape["tp"]
    torus = Mesh(mesh.devices.reshape(nz, ny, ntp), ("z", "y", "tp"))
    sp = ("z", "y")
    cut = P(sp, "tp")
    in_specs = (cut,) * 6 + (
        P("tp", None),
        P("tp"),
        P("tp", None),
        P(sp, None),
        P(),
        cut,
        cut,
        P("tp", sp),
    )
    return jax.shard_map(
        functools.partial(per_device, nz, ny, ntp),
        mesh=torus,
        in_specs=in_specs,
        out_specs=P(("z", "y", "tp"), None),
        check_vma=False,
    )


def solution(mesh):
    return build(mesh, 16, 4)
```

time: 122 us -> 106 us (0.87)
  Pallas kernels: 119 us -> 103 us
    pallas_call x1, Pallas kernels: 119 us -> 103 us  [per_device(): pl.pallas_call(functools.partial(kernel, nz, ny, ntp), out_shape=jax.Shap...]
where the time goes in v2:
time: 106 us
  Pallas kernels  103 us (97%)
  local copies, waits for them, and re-layouts  2.81 us (3%)
    pallas_call x1, Pallas kernels, per_device(): pl.pallas_call(functools.partial(kernel, nz, ny, ntp), out_shape=jax.Shap...  103 us
    unnamed x3, local copies, waits for them, and re-layouts  2.22 us

profile of v2, /device:TPU:1, one launch (start us, length us, event | category | flops | bytes accessed | tf_op | source)
XLA Modules:
  0.0 106.3 jit_solution(13647818906327878322)
XLA Ops:
  0.0 0.0 copy-start
  0.0 0.7 copy-done
  0.7 0.6 reshape.9.stw_ref
  1.3 103.5 %layer.1 = bf16[24,2048]{1,0:T(8,128)(2,1)} custom-call(bf16[192,128]{1,0:T(8,128)(2,1)} %r_ref.1, bf16[192,128]{1,0:T(8,128)(2,1)} %k_ref.1, bf16[192,128]{1,0:T(8,128)(2,1)} %v_ref.1, f32[192,128]{1,0:T(8,128)} %pre_ref.1, f32[192,128]{1,0:T(8,128)} %lr_ref.1, bf16[192,128]{1,0:T(8,128)(2,1)} %og_ref.1, f32[1,128]{1,0:T(1,128)} %reshape.9.stw_ref, ...), custom_call_target="tpu_custom_call" | custom-call | tf_op jit(solution)/shard_map/layer/pallas_call | solution.py:684
  104.7 1.5 %copy.16 = bf16[24,2048]{1,0:T(8,128)(2,1)} copy(bf16[24,2048]{1,0:T(8,128)(2,1)} %layer.1) | data formatting | bytes 196608
Async XLA Ops:
  0.0 0.7 copy-start

commit v3 on v2

--- a/solution.py
+++ b/solution.py
@@ -17,7 +17,7 @@
 BF = jnp.bfloat16
 NN = (((1,), (0,)), ((), ()))
 NT = (((1,), (1,)), ((), ()))
-SEMS = 200
+SEMS = 96
 
 
 def dg(a, b, dims=NN):
@@ -112,7 +112,6 @@
                 v=stacked(v),
             )
         )
-    yield
     for m in made:
         gram = dot_halves(m["left"], m["right"], NT)
         m["lb"] = jnp.where(strict, gram[:W2, :W2], 0.0)
@@ -123,7 +122,6 @@
     for m in made:
         m["lkv"] = dot2(m["lk"], m["vs"])
         m["mkv"] = dot2(m["mk"], m["vs"])
-    yield
     size = 1
     while size < CHUNK:
         row, col = i // size, j // size
@@ -139,8 +137,6 @@
             for m, h, x in zip(made, held, mid):
                 m["inv"] = m["inv"] + dot_halves(halves(x), h)
         size *= 2
-        if size == 8 or size == 32:
-            yield
     for m in made:
         m["tuv"] = dot3(m["inv"], jnp.concatenate([m["us"], m["lkv"]], axis=1))
     out = []
@@ -162,6 +158,21 @@
     nz,
     ny,
     ntp,
+    r_in,
+    k_in,
+    v_in,
+    pre_in,
+    lr_in,
+    og_in,
+    stw_in,
+    hg_in,
+    ow_in,
+    res_in,
+    gain_in,
+    gate_in,
+    up_in,
+    down_in,
+    out_ref,
     r_ref,
     k_ref,
     v_ref,
@@ -170,13 +181,7 @@
     og_ref,
     stw_ref,
     hg_ref,
-    ow_in,
-    res_in,
     gain_ref,
-    gate_in,
-    up_in,
-    down_in,
-    out_ref,
     gu,
     dn,
     ow,
@@ -200,13 +205,14 @@
     rsem,
 ):
     z, y, tp = lax.axis_index("z"), lax.axis_index("y"), lax.axis_index("tp")
-    rows = r_ref.shape[0]
+    rows = r_in.shape[0]
     chunks = rows // CHUNK
     own = rows // ntp
     width = res_in.shape[1]
     half_f = gate_in.shape[0]
     ff = gate_in.shape[1]
     half_ring = nz // 2
+    extra = half_f // 4
     nx = ntp // 2
     xx, core = tp // 2, tp % 2
 
@@ -236,12 +242,29 @@
             scope[0].__enter__()
 
     mark("enter")
+    here = sp(z, y)
+    weights = [
+        (gate_in, gu.at[here, 0:half_f]),
+        (up_in, gu.at[here, half_f : 2 * half_f]),
+        (down_in.at[0:extra], gu.at[here, 2 * half_f : 2 * half_f + extra]),
+        (down_in.at[extra:half_f], dn.at[here]),
+        (ow_in, ow.at[tp]),
+    ]
+    streams = [
+        (k_in, k_ref),
+        (pre_in, pre_ref),
+        (lr_in, lr_ref),
+        (r_in, r_ref),
+        (v_in, v_ref),
+        (og_in, og_ref),
+        (stw_in, stw_ref),
+        (hg_in, hg_ref),
+        (gain_in, gain_ref),
+        (res_in, res),
+    ]
     loads = [
-        pltpu.make_async_copy(gate_in, gu.at[sp(z, y), 0:half_f], lsem.at[0]),
-        pltpu.make_async_copy(up_in, gu.at[sp(z, y), half_f : 2 * half_f], lsem.at[1]),
-        pltpu.make_async_copy(down_in, dn.at[sp(z, y)], lsem.at[2]),
-        pltpu.make_async_copy(ow_in, ow.at[tp], lsem.at[3]),
-        pltpu.make_async_copy(res_in, res, lsem.at[4]),
+        pltpu.make_async_copy(src, dst, lsem.at[i])
+        for i, (src, dst) in enumerate(weights + streams)
     ]
     for load in loads:
         load.start()
@@ -253,122 +276,154 @@
     for peer in peers:
         pl.semaphore_signal(barrier, inc=1, device_id=peer, device_id_type=pl.DeviceIdType.MESH)
     pl.semaphore_wait(barrier, len(peers))
-    for load in loads:
+    for load in loads[: len(weights)]:
         load.wait()
 
     count = [0]
-    sent = []
 
     def channel():
         count[0] += 1
         return count[0] - 1
 
-    def copy(src, dst, ch, device):
+    def copy(src, dst, out, ch, device):
         return pltpu.make_async_remote_copy(
             src_ref=src,
             dst_ref=dst,
-            send_sem=ssem.at[ch],
+            send_sem=ssem.at[out],
             recv_sem=rsem.at[ch],
             device_id=device,
             device_id_type=pl.DeviceIdType.MESH,
         )
 
-    def send(ref, ch, device):
-        c = copy(ref, ref, ch, device)
-        c.start()
-        sent.append(c)
-
-    def arrived(ref, ch, device):
-        copy(ref, ref, ch, device).wait_recv()
+    GU, DN, PS, PY, OW, MX, PART, COMB = range(8)
+
+    def send(ref, out, ch, device):
+        copy(ref, ref, out, ch, device).start()
+
+    def arrived(ref, ch):
+        copy(ref, ref, 0, ch, dev(zz=zof(1))).wait_recv()
 
     class Ring:
-        def __init__(self, block):
-            self.block = block
-            self.ch = [(channel(), channel()) for _ in range(half_ring)]
+        def __init__(self, block, out, one, two):
+            self.block, self.out, self.one, self.two = block, out, one, two
+            self.ch = [channel() for _ in range(half_ring)]
             self.step = 1
 
         def piece(self, s, side):
             return side if s == half_ring else None
 
         def push(self, s):
-            send(self.block(zof(1 - s), self.piece(s, 0)), self.ch[s - 1][0], dev(zz=zof(1)))
-            send(self.block(zof(s - 1), self.piece(s, 1)), self.ch[s - 1][1], dev(zz=zof(-1)))
+            ch = self.ch[s - 1]
+            send(self.block(zof(1 - s), self.piece(s, 0)), self.out, ch, dev(zz=zof(1)))
+            send(self.block(zof(s - 1), self.piece(s, 1)), self.out, ch, dev(zz=zof(-1)))
 
         def turn(self):
             s = self.step
             if s > half_ring:
                 return
-            arrived(self.block(zof(-s), self.piece(s, 0)), self.ch[s - 1][0], dev(zz=zof(-1)))
-            arrived(self.block(zof(s), self.piece(s, 1)), self.ch[s - 1][1], dev(zz=zof(1)))
+            arrived(self.one if s == half_ring else self.two, self.ch[s - 1])
             if s < half_ring:
                 self.push(s + 1)
             self.step = s + 1
 
+    class PairRing:
+        def __init__(self):
+            self.ch = [(channel(), channel()) for _ in range(half_ring)]
+
+        def part(self, zz, half):
+            return pz.at[zz, half * HS : (half + 1) * HS]
+
+        def push(self, s, half):
+            ch = self.ch[s - 1][half]
+            if s < half_ring or half == 0:
+                send(self.part(zof(1 - s), half), PS, ch, dev(zz=zof(1)))
+            if s < half_ring or half == 1:
+                send(self.part(zof(s - 1), half), PS, ch, dev(zz=zof(-1)))
+
+        def turn(self, s):
+            for half in range(2):
+                arrived(pz.at[0] if s < half_ring else self.part(0, half), self.ch[s - 1][half])
+                if s < half_ring:
+                    self.push(s + 1, half)
+
     class Across:
-        def __init__(self, block, at, to):
-            self.block, self.at, self.to = block, at, to
-            self.ch = [channel() for _ in range(4)]
+        def __init__(self, block, at, to, out, one, two, last=None):
+            self.block, self.at, self.to, self.out = block, at, to, out
+            self.one, self.two = one, two
+            self.first = channel()
+            self.last = channel() if last is None else last
 
         def push(self):
-            send(self.block(self.at(0), None), self.ch[0], self.to(1))
-            send(self.block(self.at(0), None), self.ch[1], self.to(-1))
+            send(self.block(self.at(0), None), self.out, self.first, self.to(1))
+            send(self.block(self.at(0), None), self.out, self.first, self.to(-1))
 
         def forward(self):
-            arrived(self.block(self.at(-1), None), self.ch[0], self.to(-1))
-            send(self.block(self.at(-1), 0), self.ch[2], self.to(1))
-            arrived(self.block(self.at(1), None), self.ch[1], self.to(1))
-            send(self.block(self.at(1), 1), self.ch[3], self.to(-1))
+            arrived(self.two, self.first)
+            send(self.block(self.at(-1), 0), self.out, self.last, self.to(1))
+            send(self.block(self.at(1), 1), self.out, self.last, self.to(-1))
 
         def finish(self):
-            arrived(self.block(self.at(2), 0), self.ch[2], self.to(-1))
-            arrived(self.block(self.at(2), 1), self.ch[3], self.to(1))
-
-    def cut(ref, piece, size):
-        return ref if piece is None else ref.at[piece * size : (piece + 1) * size]
+            arrived(self.one, self.last)
+
+    def cut(ref, piece, length):
+        if piece is None:
+            return ref
+        middle = (length // 2 + 7) // 8 * 8
+        return ref.at[0:middle] if piece == 0 else ref.at[middle:length]
+
+    a_rows = 2 * half_f + extra
+    b_rows = half_f - extra
 
     def gu_block(zz, yy, piece):
-        return cut(gu.at[sp(zz, yy)], piece, half_f)
-
-    def dn_pair(which, zz, piece):
-        if piece is None:
-            return dn.at[pl.ds(zz * ny + which * (ny // 2), ny // 2)]
-        return dn.at[pl.ds(zz * ny + which * (ny // 2) + piece * (ny // 4), ny // 4)]
+        return cut(gu.at[sp(zz, yy)], piece, a_rows)
+
+    def dn_block(zz, yy, piece):
+        return cut(dn.at[sp(zz, yy)], piece, b_rows)
 
     def y_dev(d):
         return dev(yy=yof(d))
 
-    ring_gu = Ring(lambda zz, piece: gu_block(zz, y, piece))
-    ring_d0 = Ring(functools.partial(dn_pair, 0))
-    ring_d1 = Ring(functools.partial(dn_pair, 1))
-    ring_ps = Ring(lambda zz, piece: cut(pz.at[zz], piece, HS))
+    ring_gu = Ring(lambda zz, piece: gu_block(zz, y, piece), GU, gu.at[0], gu.at[0:2])
+    ring_dn = [
+        Ring(
+            functools.partial(lambda k, zz, piece: dn_block(zz, yof(k), piece), k),
+            DN,
+            dn.at[0],
+            dn.at[0:2],
+        )
+        for k in (0, 1, -1, 2)
+    ]
+    ring_ps = PairRing()
     order = [0]
     for s in range(1, half_ring):
         order += [-s, s]
     order += [half_ring]
+    far_halves = channel()
     across = [
         Across(
             functools.partial(lambda step, yy, piece: gu_block(zof(step), yy, piece), step),
             yof,
             y_dev,
+            GU,
+            gu.at[0:nz],
+            gu.at[0:2],
+            far_halves,
         )
         for step in order
     ]
-    across_dn = Across(lambda yy, piece: cut(dn.at[sp(z, yy)], piece, half_f // 2), yof, y_dev)
-
-    bulk = [ring_gu] * 3 + [ring_d0]
-    while len(bulk) < 3 * half_ring:
-        bulk += [ring_d1, ring_gu, ring_d0]
-    bulk += [ring_d1] * half_ring + [ring_d0] * half_ring
-    progress = {"bulk": 0, "push": 1, "forward": 0}
-
-    def turn(n=1):
-        done = 0
-        while done < n and progress["bulk"] < len(bulk):
-            ring = bulk[progress["bulk"]]
-            progress["bulk"] += 1
-            if ring.step <= half_ring:
-                ring.turn()
-                done += 1
+    across_dn = Across(
+        lambda yy, piece: dn_block(z, yy, piece), yof, y_dev, DN, dn.at[0], dn.at[0:2]
+    )
+
+    progress = {"push": 1, "forward": 0, "dn": 0}
+
+    def turn_gu():
+        ring_gu.turn()
+
+    def turn_dn(n=1):
+        for _ in range(n):
+            ring_dn[progress["dn"] % 4].turn()
+            progress["dn"] += 1
 
     def y_push(n=1):
         for _ in range(n):
@@ -396,20 +451,27 @@
     near = dev(tt=partner)
     across_ow = None
     if nx == 4:
-        across_ow = Across(lambda t, piece: cut(ow.at[t], piece, W2 // 2), same_core, x_dev)
-    ow_far = [channel() for _ in range(1, nx)]
-    ow_near = [channel() for _ in range(nx)]
+        across_ow = Across(
+            lambda t, piece: cut(ow.at[t], piece, W2),
+            same_core,
+            x_dev,
+            OW,
+            ow.at[0],
+            ow.at[0:2],
+        )
+    ow_far = [channel() for _ in range(1, nx)] if across_ow is None else []
+    ow_near = channel()
+
+    def ow_share(d):
+        send(ow.at[same_core(d)], OW, ow_near, near)
 
     def ow_start():
         if across_ow is not None:
             across_ow.push()
         else:
             for d in range(1, nx):
-                send(ow.at[tp], ow_far[d - 1], x_dev(d))
-        send(ow.at[tp], ow_near[0], near)
-
-    def ow_share(d):
-        send(ow.at[same_core(d)], ow_near[d % nx], near)
+                send(ow.at[tp], OW, ow_far[d - 1], x_dev(d))
+        ow_share(0)
 
     def ow_middle():
         if across_ow is not None:
@@ -423,18 +485,20 @@
             ow_share(2)
         else:
             for d in range(1, nx):
-                arrived(ow.at[same_core(-d)], ow_far[d - 1], x_dev(-d))
+                arrived(ow.at[0], ow_far[d - 1])
                 ow_share(-d)
 
     def ow_finish():
-        for d in range(nx):
-            arrived(ow.at[other_core(d)], ow_near[d], near)
+        arrived(ow.at[0:nx], ow_near)
 
     mark("launch")
     ring_gu.push(1)
+    ring_dn[0].push(1)
+    across_dn.push()
     across[0].push()
-    across_dn.push()
     ow_start()
+    for load in loads[len(weights) :]:
+        load.wait()
 
     mark("recur")
     ones = head_ones()
@@ -443,25 +507,7 @@
     for span in spans:
         r, k, v = (ref[span, :].astype(F32) for ref in (r_ref, k_ref, v_ref))
         given.append((r, k, v, pre_ref[span, :], lr_ref[span, :]))
-    stages = chunk_stages(given)
-    stage = 0
-    while True:
-        try:
-            next(stages)
-        except StopIteration as end:
-            made = end.value
-            break
-        mark(f"recur_pump{stage}")
-        if stage == 1:
-            turn()
-            y_push()
-        if stage == 2:
-            across_dn.forward()
-        if stage == 3:
-            turn()
-            y_forward()
-        stage += 1
-        mark(f"recur{stage}")
+    made = chunk_stages(given)
     pair = None
     for c, (ps, seen, local) in enumerate(made):
         seen_ref[spans[c], :] = seen
@@ -471,19 +517,26 @@
             entry[c] = pair
     mark("scan_y")
     py[y] = pair
-    ch_y = [channel() for _ in range(1, ny)]
-    for d in range(1, ny):
-        send(py.at[y], ch_y[d - 1], dev(yy=yof(d)))
-    y_push(2)
-    across_dn.finish()
-    ring_d0.push(1)
+    ch_y = channel()
+    for d in (2, 1, 3) if ny == 4 else range(1, ny):
+        send(py.at[y], PY, ch_y, dev(yy=yof(d)))
+    mark("pre_gu")
+    turn_gu()
+    mark("pre_dn")
+    ring_dn[0].turn()
+    mark("pre_dny")
+    across_dn.forward()
+    ring_dn[1].push(1)
+    ring_dn[2].push(1)
+    stw = stw_ref[...]
+    stw = jnp.concatenate([stw[0:1], stw[1:2]], axis=1)
     for c, (r, k, v, _, _) in enumerate(given):
-        self_ref[spans[c], :] = dot2(r * k * stw_ref[...], ones) * v
-    turn()
+        self_ref[spans[c], :] = dot2(r * k * stw, ones) * v
+    mark("pre_y0")
+    y_forward()
+    y_push()
     mark("scan_ywait")
-    ring_d1.push(1)
-    for d in range(1, ny):
-        arrived(py.at[yof(-d)], ch_y[d - 1], dev(yy=yof(-d)))
+    arrived(py.at[0 : ny - 1], ch_y)
     mark("scan_yfix")
     inside = identity_pair()
     running = py[0]
@@ -491,17 +544,30 @@
         inside = jnp.where(y == yy, running, inside)
         running = compose(running, py[yy])
     pz[z] = running
-    ring_ps.push(1)
+    ring_ps.push(1, 0)
+    ring_ps.push(1, 1)
+    mark("pre_dn2")
+    across_dn.finish()
+    ring_dn[3].push(1)
+    y_push()
+    progress["dn"] = 1
 
     trans_left = identity_pair()[:HS]
     state_left = jnp.zeros((HS, W2), F32)
     state_right = jnp.zeros((HS, W2), F32)
     for s in range(1, half_ring + 1):
         mark(f"scan_z{s}")
-        turn()
-        ring_ps.turn()
+        ring_ps.turn(s)
+        mark(f"bulk{s}")
+        if s % 2 == 1:
+            turn_gu()
+            turn_dn()
+        else:
+            turn_dn(3)
         y_push()
+        mark(f"yfwd{s}")
         y_forward()
+        mark(f"calc{s}")
         if s == half_ring // 2:
             ow_middle()
         if s == half_ring - 1:
@@ -521,6 +587,8 @@
     state = dot3(state_right, stacked(trans_left)) + state_left
     state = dot3(state, stacked(inside[:HS])) + inside[HS:]
 
+    turn_gu()
+    y_push()
     mark("mech")
     for c in range(chunks):
         span = spans[c]
@@ -535,27 +603,30 @@
         gated = merged * jax.nn.sigmoid(og_ref[span, :].astype(F32))
         mx[tp, span, :] = gated.astype(BF)
     mx_far = [channel() for _ in range(1, nx)]
-    mx_near = [channel() for _ in range(nx)]
+    mx_near = channel()
     for d in range(1, nx):
-        send(mx.at[tp], mx_far[d - 1], x_dev(d))
-    send(mx.at[tp], mx_near[0], near)
+        send(mx.at[tp], MX, mx_far[d - 1], x_dev(d))
+    send(mx.at[tp], MX, mx_near, near)
     mark("exch_pump")
-    turn(2)
+    turn_dn(3)
     y_push()
     y_forward()
     mark("exch_far")
     for d in range(1, nx):
-        slot = mx.at[same_core(-d)]
-        arrived(slot, mx_far[d - 1], x_dev(-d))
-        send(slot, mx_near[d], near)
+        arrived(mx.at[0], mx_far[d - 1])
+        send(mx.at[same_core(-d)], MX, mx_near, near)
+    mark("exch_pump2")
+    turn_gu()
+    y_push()
+    turn_dn()
+    y_forward()
     mark("exch_near")
-    for d in range(nx):
-        arrived(mx.at[other_core(-d)], mx_near[d], near)
+    arrived(mx.at[0:nx], mx_near)
     mark("exch_ow")
     ow_finish()
-    mark("exch_pump2")
-    turn(2)
-    y_push()
+    mark("exch_pump3")
+    turn_dn(3)
+    y_push(2)
     y_forward()
 
     mark("project")
@@ -576,6 +647,10 @@
     square = jnp.zeros((rows, W2), F32)
     square = lax.fori_loop(0, tiles, project, square)
     mark("norm")
+    turn_gu()
+    y_push(2)
+    turn_dn(2)
+    y_forward()
     scale = lax.rsqrt(jnp.sum(square, axis=1, keepdims=True) * (1.0 / width) + NORM_EPS)
 
     def normalize(n, carry):
@@ -586,12 +661,12 @@
     lax.fori_loop(0, tiles, normalize, 0)
     mark("pumprest")
     while progress["forward"] < len(across):
-        turn()
+        turn_gu()
         y_push(2)
+        turn_dn(2)
         y_forward()
     mark("finish")
-    for a in across:
-        a.finish()
+    across[0].finish()
 
     mark("gateup")
     at = 0
@@ -602,55 +677,68 @@
         up = dg(x, gu[:, half_f : 2 * half_f, at : at + wide].reshape(width, wide))
         hid[:, at : at + wide] = (gate / (1.0 + jnp.exp(-gate)) * up).astype(BF)
         at += wide
-        turn()
+        turn_dn(2)
     mark("dnwait")
-    turn(3 * half_ring)
+    turn_dn(4 * half_ring)
 
     slots = tile // half_f
     half_w = width // 2
 
     def down(n, carry):
         cols = pl.ds(pl.multiple_of(n * tile, tile), tile)
-        w = dn[pl.ds(n * slots, slots)].reshape(tile, ff)
+        these = pl.ds(n * slots, slots)
+        first = gu[these, 2 * half_f : 2 * half_f + extra, :]
+        w = jnp.concatenate([first, dn[these]], axis=1).reshape(tile, ff)
         prod = dg(hid[...], w, NT).reshape(nx, 2, own, tile).astype(BF)
         part[0, :, :, cols] = prod[:, 0]
         part[1, :, :, cols] = prod[:, 1]
         return carry
 
-    def pass_on(src, dst, ch, device):
-        c = copy(src, dst, ch, device)
-        c.start()
-        sent.append(c)
-
     pieces = [pl.ds(piece * half_w, half_w) for piece in range(2)]
     ch_core = [channel() for _ in range(2)]
-    ch_part = [[channel() for _ in range(1, nx)] for _ in range(2)]
+    ch_part = [channel() for _ in range(2)]
     for piece, cols in enumerate(pieces):
         mark(f"down{piece}")
         lax.fori_loop(piece * tiles // 2, (piece + 1) * tiles // 2, down, 0)
-        pass_on(part.at[1 - core, :, :, cols], pgot.at[:, :, cols], ch_core[piece], near)
+        copy(
+            part.at[1 - core, :, :, cols], pgot.at[:, :, cols], PART, ch_core[piece], near
+        ).start()
 
     def x_at(d):
         return lax.rem(xx + d + nx, nx)
 
     for piece, cols in enumerate(pieces):
         mark(f"rs_core{piece}")
-        arrived(pgot.at[:, :, cols], ch_core[piece], near)
+        arrived(pgot.at[:, :, cols], ch_core[piece])
         for d in [2, 1, 3] if nx == 4 else range(1, nx):
             both = part[core, x_at(d), :, cols].astype(F32) + pgot[x_at(d), :, cols].astype(F32)
             comb[d - 1, :, cols] = both.astype(BF)
-            pass_on(comb.at[d - 1, :, cols], got.at[d - 1, :, cols], ch_part[piece][d - 1], x_dev(d))
+            copy(
+                comb.at[d - 1, :, cols], got.at[d - 1, :, cols], COMB, ch_part[piece], x_dev(d)
+            ).start()
     mark("rs_wait")
     for piece, cols in enumerate(pieces):
         total = am[pl.ds(pl.multiple_of(tp * own, own), own), cols]
         total = total + part[core, xx, :, cols].astype(F32) + pgot[xx, :, cols].astype(F32)
+        if nx > 1:
+            arrived(got.at[:, :, cols], ch_part[piece])
         for d in range(1, nx):
-            arrived(got.at[d - 1, :, cols], ch_part[piece][d - 1], x_dev(-d))
             total = total + got[d - 1, :, cols].astype(F32)
         out_ref[:, cols] = total.astype(BF)
     mark("sendwait")
-    for c in sent:
-        c.wait_send()
+    gone = [
+        (gu.at[0 : nz * ny - 1], GU),
+        (dn.at[0 : nz * ny - 1], DN),
+        (pz.at[0 : nz - 1], PS),
+        (py.at[0 : ny - 1], PY),
+        (ow.at[0 : ntp - 1], OW),
+        (mx.at[0 : ntp - 1], MX),
+        (part.at[0], PART),
+    ]
+    if nx > 1:
+        gone.append((comb, COMB))
+    for ref, out in gone:
+        copy(ref, ref, out, 0, near).wait_send()
     mark(None)
     assert count[0] <= SEMS, count[0]
 
@@ -684,11 +772,20 @@
     return pl.pallas_call(
         functools.partial(kernel, nz, ny, ntp),
         out_shape=jax.ShapeDtypeStruct((own, width), BF),
-        in_specs=[vmem] * 8 + [hbm, hbm, vmem, hbm, hbm, hbm],
+        in_specs=[hbm] * 14,
         out_specs=vmem,
         scratch_shapes=[
-            pltpu.VMEM((nz * ny, 2 * half_f, ff), BF),
-            pltpu.VMEM((nz * ny, half_f, ff), BF),
+            pltpu.VMEM((rows, W2), BF),
+            pltpu.VMEM((rows, W2), BF),
+            pltpu.VMEM((rows, W2), BF),
+            pltpu.VMEM((rows, W2), F32),
+            pltpu.VMEM((rows, W2), F32),
+            pltpu.VMEM((rows, W2), BF),
+            pltpu.VMEM((2, HS), F32),
+            pltpu.VMEM((1, W2), F32),
+            pltpu.VMEM((1, width), F32),
+            pltpu.VMEM((nz * ny, 2 * half_f + half_f // 4, ff), BF),
+            pltpu.VMEM((nz * ny, half_f - half_f // 4, ff), BF),
             pltpu.VMEM((ntp, W2, width), BF),
             pltpu.VMEM((rows, width), BF),
             pltpu.VMEM((ny, W2, W2), F32),
@@ -705,8 +802,8 @@
             pltpu.VMEM((max(nx - 1, 1), own, width), BF),
             pltpu.VMEM((nx, own, width), BF),
             pltpu.VMEM((max(nx - 1, 1), own, width), BF),
-            pltpu.SemaphoreType.DMA((5,)),
-            pltpu.SemaphoreType.DMA((SEMS,)),
+            pltpu.SemaphoreType.DMA((15,)),
+            pltpu.SemaphoreType.DMA((8,)),
             pltpu.SemaphoreType.DMA((SEMS,)),
         ],
         compiler_params=pltpu.CompilerParams(
@@ -720,7 +817,7 @@
         decay_preact,
         learning_rate_preact,
         output_gate_preact,
-        self_token_weight.reshape(1, -1),
+        self_token_weight,
         head_norm_gain.reshape(1, -1),
         output_weight,
         residual,

time: 106 us -> 89.9 us (0.85)
  Pallas kernels: 103 us -> 88.2 us
  local copies, waits for them, and re-layouts: 2.81 us -> 1.54 us
    pallas_call x1, Pallas kernels: 103 us -> 88.2 us  [per_device(): pl.pallas_call(functools.partial(kernel, nz, ny, ntp), out_shape=jax.Shap...]
    unnamed x3 -> x1, local copies, waits for them, and re-layouts: 2.22 us -> 1.54 us
where the time goes in v3:
time: 89.9 us; the launch traced here: 89.8 us
  Pallas kernels  88.2 us (98%)
  local copies, waits for them, and re-layouts  1.54 us (2%)
    pallas_call x1, Pallas kernels, per_device(): pl.pallas_call(functools.partial(kernel, nz, ny, ntp), out_shape=jax.Shap...  88.2 us

profile of v3, /device:TPU:1, one launch (start us, length us, event | category | flops | bytes accessed | tf_op | source)
XLA Modules:
  0.0 89.8 jit_solution(7225067097337678438)
XLA Ops:
  0.0 88.2 %layer.1 = bf16[24,2048]{1,0:T(8,128)(2,1)} custom-call(bf16[192,128]{1,0:T(8,128)(2,1)} %r_in.1, bf16[192,128]{1,0:T(8,128)(2,1)} %k_in.1, bf16[192,128]{1,0:T(8,128)(2,1)} %v_in.1, f32[192,128]{1,0:T(8,128)} %pre_in.1, f32[192,128]{1,0:T(8,128)} %lr_in.1, bf16[192,128]{1,0:T(8,128)(2,1)} %og_in.1, f32[2,64]{1,0:T(2,128)} %stw_in.1, f32[1,128]{1,0:T(1,128)} %bitcast.5, ...), custom_call_target="tpu_custom_call" | custom-call | tf_op jit(solution)/shard_map/layer/pallas_call | solution.py:772
  88.2 1.5 %copy.16 = bf16[24,2048]{1,0:T(8,128)(2,1)} copy(bf16[24,2048]{1,0:T(8,128)(2,1)} %layer.1) | data formatting | bytes 196608

commit v4 on v3

--- a/solution.py
+++ b/solution.py
@@ -68,13 +68,10 @@
 
 
 def compose(earlier, later):
-    moved = dot3(earlier, stacked(later[:HS]))
-    return jnp.concatenate([moved[:HS], moved[HS:] + later[HS:]], axis=0)
-
-
-def identity_pair():
+    later_d = stacked(later[:HS])
     i, j = iota((W2, W2), 0), iota((W2, W2), 1)
-    return ((i == j) | (i + HS == j)).astype(F32) * (i < HS).astype(F32)
+    moved = dot3(earlier, later_d + (i == j).astype(F32))
+    return jnp.concatenate([moved[:HS] + later[:HS], moved[HS:] + later[HS:]], axis=0)
 
 
 def chunk_stages(chunks):
@@ -119,6 +116,7 @@
         m["mb"] = jnp.where(incl, gram[W2:, :W2], 0.0)
         m["mk"] = jnp.where(incl, gram[W2:, W2:], 0.0)
         m["vs"] = m["v"].astype(BF)
+    yield
     for m in made:
         m["lkv"] = dot2(m["lk"], m["vs"])
         m["mkv"] = dot2(m["mk"], m["vs"])
@@ -142,7 +140,7 @@
     out = []
     for m in made:
         turned = dot_halves(halves(m["tuv"].T), m["bts"])
-        trans = folded(jnp.where(i == j, jnp.exp(m["last"]), 0.0) + turned[:W2])
+        trans = folded(jnp.where(i == j, jnp.exp(m["last"]) - 1.0, 0.0) + turned[:W2])
         vt = m["v"].T.astype(BF)
         state = folded(turned[W2:] + dg(vt, m["kts"][0]) + dg(vt, m["kts"][1]))
         m["pair"] = jnp.concatenate([trans, state], axis=0)
@@ -212,7 +210,6 @@
     half_f = gate_in.shape[0]
     ff = gate_in.shape[1]
     half_ring = nz // 2
-    extra = half_f // 4
     nx = ntp // 2
     xx, core = tp // 2, tp % 2
 
@@ -246,13 +243,12 @@
     weights = [
         (gate_in, gu.at[here, 0:half_f]),
         (up_in, gu.at[here, half_f : 2 * half_f]),
-        (down_in.at[0:extra], gu.at[here, 2 * half_f : 2 * half_f + extra]),
-        (down_in.at[extra:half_f], dn.at[here]),
+        (down_in, dn.at[here]),
         (ow_in, ow.at[tp]),
     ]
     streams = [
+        (pre_in, pre_ref),
         (k_in, k_ref),
-        (pre_in, pre_ref),
         (lr_in, lr_ref),
         (r_in, r_ref),
         (v_in, v_ref),
@@ -266,7 +262,7 @@
         pltpu.make_async_copy(src, dst, lsem.at[i])
         for i, (src, dst) in enumerate(weights + streams)
     ]
-    for load in loads:
+    for load in loads[len(weights) :] + loads[: len(weights)]:
         load.start()
 
     barrier = pltpu.get_barrier_semaphore()
@@ -275,6 +271,18 @@
     peers += [dev(tt=tof(d)) for d in range(1, ntp)]
     for peer in peers:
         pl.semaphore_signal(barrier, inc=1, device_id=peer, device_id_type=pl.DeviceIdType.MESH)
+    early = len(weights) + 5
+    for load in loads[len(weights) : early]:
+        load.wait()
+    mark("recur_a")
+    spans = [pl.ds(c * CHUNK, CHUNK) for c in range(chunks)]
+    given = []
+    for span in spans:
+        r, k, v = (ref[span, :].astype(F32) for ref in (r_ref, k_ref, v_ref))
+        given.append((r, k, v, pre_ref[span, :], lr_ref[span, :]))
+    stages = chunk_stages(given)
+    next(stages)
+    mark("greet")
     pl.semaphore_wait(barrier, len(peers))
     for load in loads[: len(weights)]:
         load.wait()
@@ -371,8 +379,8 @@
         middle = (length // 2 + 7) // 8 * 8
         return ref.at[0:middle] if piece == 0 else ref.at[middle:length]
 
-    a_rows = 2 * half_f + extra
-    b_rows = half_f - extra
+    a_rows = 2 * half_f
+    b_rows = half_f
 
     def gu_block(zz, yy, piece):
         return cut(gu.at[sp(zz, yy)], piece, a_rows)
@@ -497,17 +505,15 @@
     across_dn.push()
     across[0].push()
     ow_start()
-    for load in loads[len(weights) :]:
+    for load in loads[early:]:
         load.wait()
 
     mark("recur")
     ones = head_ones()
-    spans = [pl.ds(c * CHUNK, CHUNK) for c in range(chunks)]
-    given = []
-    for span in spans:
-        r, k, v = (ref[span, :].astype(F32) for ref in (r_ref, k_ref, v_ref))
-        given.append((r, k, v, pre_ref[span, :], lr_ref[span, :]))
-    made = chunk_stages(given)
+    try:
+        next(stages)
+    except StopIteration as end:
+        made = end.value
     pair = None
     for c, (ps, seen, local) in enumerate(made):
         seen_ref[spans[c], :] = seen
@@ -516,7 +522,7 @@
         if c < chunks - 1:
             entry[c] = pair
     mark("scan_y")
-    py[y] = pair
+    py[y] = pair.astype(BF)
     ch_y = channel()
     for d in (2, 1, 3) if ny == 4 else range(1, ny):
         send(py.at[y], PY, ch_y, dev(yy=yof(d)))
@@ -526,8 +532,6 @@
     ring_dn[0].turn()
     mark("pre_dny")
     across_dn.forward()
-    ring_dn[1].push(1)
-    ring_dn[2].push(1)
     stw = stw_ref[...]
     stw = jnp.concatenate([stw[0:1], stw[1:2]], axis=1)
     for c, (r, k, v, _, _) in enumerate(given):
@@ -538,35 +542,38 @@
     mark("scan_ywait")
     arrived(py.at[0 : ny - 1], ch_y)
     mark("scan_yfix")
-    inside = identity_pair()
-    running = py[0]
+    inside = jnp.zeros((W2, W2), F32)
+    running = py[0].astype(F32)
     for yy in range(1, ny):
         inside = jnp.where(y == yy, running, inside)
-        running = compose(running, py[yy])
-    pz[z] = running
+        running = compose(running, py[yy].astype(F32))
+    pz[z] = running.astype(BF)
     ring_ps.push(1, 0)
     ring_ps.push(1, 1)
     mark("pre_dn2")
+    ring_dn[1].push(1)
+    ring_dn[2].push(1)
     across_dn.finish()
     ring_dn[3].push(1)
-    y_push()
+    turn_gu()
+    y_push(2)
     progress["dn"] = 1
 
-    trans_left = identity_pair()[:HS]
+    trans_left = jnp.zeros((HS, W2), F32)
     state_left = jnp.zeros((HS, W2), F32)
     state_right = jnp.zeros((HS, W2), F32)
     for s in range(1, half_ring + 1):
         mark(f"scan_z{s}")
         ring_ps.turn(s)
         mark(f"bulk{s}")
-        if s % 2 == 1:
+        if s in (1, 2, 4, 6, 7):
             turn_gu()
-            turn_dn()
+            turn_dn(2)
         else:
-            turn_dn(3)
-        y_push()
+            turn_dn(4)
+        y_push(2)
         mark(f"yfwd{s}")
-        y_forward()
+        y_forward(2 if s % 2 == 0 else 1)
         mark(f"calc{s}")
         if s == half_ring // 2:
             ow_middle()
@@ -574,63 +581,60 @@
             ow_last()
         left = pz[zof(-s)]
         has_left = z >= s
-        moved = dot3(left, stacked(trans_left))
-        trans_left = jnp.where(has_left, moved[:HS], trans_left)
+        hi, lo = halves(stacked(trans_left))
+        moved = dg(left, hi) + dg(left, lo) + left.astype(F32)
+        trans_left = jnp.where(has_left, trans_left + moved[:HS], trans_left)
         state_left = jnp.where(has_left, state_left + moved[HS:], state_left)
         if s < half_ring:
-            right = pz[zof(s)]
+            right = pz[zof(s)].astype(F32)
             has_right = z + s >= nz
-            state_right = jnp.where(
-                has_right, dot3(state_right, stacked(right[:HS])) + right[HS:], state_right
-            )
+            moved = dot2(state_right, stacked(right[:HS]).astype(BF)) + right[HS:]
+            state_right = jnp.where(has_right, state_right + moved, state_right)
     mark("state")
-    state = dot3(state_right, stacked(trans_left)) + state_left
-    state = dot3(state, stacked(inside[:HS])) + inside[HS:]
+    state = state_right + dot3(state_right, stacked(trans_left)) + state_left
+    state = state + dot3(state, stacked(inside[:HS])) + inside[HS:]
 
     turn_gu()
-    y_push()
+    y_push(2)
+    turn_dn(1)
     mark("mech")
+    seen = []
     for c in range(chunks):
-        span = spans[c]
         at = state
         if c > 0:
-            at = dot3(state, stacked(entry[c - 1][:HS])) + entry[c - 1][HS:]
-        o = dot3(seen_ref[span, :], stacked(at), NT) + local_ref[span, :]
-        centre = dot2(o, ones) * (1.0 / HS)
-        shifted = o - centre
-        spread = dot2(shifted * shifted, ones) * (1.0 / HS)
-        merged = shifted * lax.rsqrt(spread + GROUP_EPS) * hg_ref[...] + self_ref[span, :]
-        gated = merged * jax.nn.sigmoid(og_ref[span, :].astype(F32))
-        mx[tp, span, :] = gated.astype(BF)
+            at = state + dot3(state, stacked(entry[c - 1][:HS])) + entry[c - 1][HS:]
+        seen.append(dot3(seen_ref[spans[c], :], stacked(at), NT))
+    o = jnp.concatenate(seen, axis=0) + local_ref[...]
+    shifted = o - dot2(o, ones) * (1.0 / HS)
+    spread = dot2(shifted * shifted, ones) * (1.0 / HS)
+    merged = shifted * lax.rsqrt(spread + GROUP_EPS) * hg_ref[...] + self_ref[...]
+    mx[tp] = (merged * jax.nn.sigmoid(og_ref[...].astype(F32))).astype(BF)
     mx_far = [channel() for _ in range(1, nx)]
     mx_near = channel()
-    for d in range(1, nx):
+    x_order = [2, 1, 3] if nx == 4 else list(range(1, nx))
+    for d in x_order:
         send(mx.at[tp], MX, mx_far[d - 1], x_dev(d))
     send(mx.at[tp], MX, mx_near, near)
     mark("exch_pump")
+    y_forward()
     turn_dn(3)
-    y_push()
-    y_forward()
     mark("exch_far")
-    for d in range(1, nx):
+    for d in reversed(x_order):
         arrived(mx.at[0], mx_far[d - 1])
         send(mx.at[same_core(-d)], MX, mx_near, near)
     mark("exch_pump2")
-    turn_gu()
-    y_push()
-    turn_dn()
     y_forward()
+    turn_dn(3)
     mark("exch_near")
     arrived(mx.at[0:nx], mx_near)
     mark("exch_ow")
     ow_finish()
     mark("exch_pump3")
-    turn_dn(3)
     y_push(2)
     y_forward()
 
     mark("project")
-    tile = min(256, width)
+    tile = min(256, width // 4)
     tiles = width // tile
     lhs = jnp.concatenate([mx[g] for g in range(ntp)], axis=1)
 
@@ -645,12 +649,13 @@
         return square
 
     square = jnp.zeros((rows, W2), F32)
-    square = lax.fori_loop(0, tiles, project, square)
+    square = lax.fori_loop(0, tiles, project, square, unroll=2)
     mark("norm")
-    turn_gu()
     y_push(2)
-    turn_dn(2)
     y_forward()
+    turn_dn(1)
+    y_forward()
+    turn_dn(1)
     scale = lax.rsqrt(jnp.sum(square, axis=1, keepdims=True) * (1.0 / width) + NORM_EPS)
 
     def normalize(n, carry):
@@ -663,8 +668,8 @@
     while progress["forward"] < len(across):
         turn_gu()
         y_push(2)
-        turn_dn(2)
         y_forward()
+        turn_dn()
     mark("finish")
     across[0].finish()
 
@@ -682,33 +687,26 @@
     turn_dn(4 * half_ring)
 
     slots = tile // half_f
-    half_w = width // 2
 
     def down(n, carry):
         cols = pl.ds(pl.multiple_of(n * tile, tile), tile)
-        these = pl.ds(n * slots, slots)
-        first = gu[these, 2 * half_f : 2 * half_f + extra, :]
-        w = jnp.concatenate([first, dn[these]], axis=1).reshape(tile, ff)
+        w = dn[pl.ds(n * slots, slots)].reshape(tile, ff)
         prod = dg(hid[...], w, NT).reshape(nx, 2, own, tile).astype(BF)
         part[0, :, :, cols] = prod[:, 0]
         part[1, :, :, cols] = prod[:, 1]
         return carry
 
-    pieces = [pl.ds(piece * half_w, half_w) for piece in range(2)]
-    ch_core = [channel() for _ in range(2)]
-    ch_part = [channel() for _ in range(2)]
-    for piece, cols in enumerate(pieces):
-        mark(f"down{piece}")
-        lax.fori_loop(piece * tiles // 2, (piece + 1) * tiles // 2, down, 0)
-        copy(
-            part.at[1 - core, :, :, cols], pgot.at[:, :, cols], PART, ch_core[piece], near
-        ).start()
+    cuts = 4
+    quarter = width // cuts
+    pieces = [pl.ds(piece * quarter, quarter) for piece in range(cuts)]
+    ch_core = [channel() for _ in range(cuts)]
+    ch_part = [channel() for _ in range(cuts)]
 
     def x_at(d):
         return lax.rem(xx + d + nx, nx)
 
-    for piece, cols in enumerate(pieces):
-        mark(f"rs_core{piece}")
+    def add_cores(piece):
+        cols = pieces[piece]
         arrived(pgot.at[:, :, cols], ch_core[piece])
         for d in [2, 1, 3] if nx == 4 else range(1, nx):
             both = part[core, x_at(d), :, cols].astype(F32) + pgot[x_at(d), :, cols].astype(F32)
@@ -716,6 +714,18 @@
             copy(
                 comb.at[d - 1, :, cols], got.at[d - 1, :, cols], COMB, ch_part[piece], x_dev(d)
             ).start()
+
+    for piece, cols in enumerate(pieces):
+        mark(f"down{piece}")
+        lax.fori_loop(piece * tiles // cuts, (piece + 1) * tiles // cuts, down, 0, unroll=True)
+        copy(
+            part.at[1 - core, :, :, cols], pgot.at[:, :, cols], PART, ch_core[piece], near
+        ).start()
+        if piece >= 2:
+            add_cores(piece - 2)
+    mark("rs_core")
+    add_cores(cuts - 2)
+    add_cores(cuts - 1)
     mark("rs_wait")
     for piece, cols in enumerate(pieces):
         total = am[pl.ds(pl.multiple_of(tp * own, own), own), cols]
@@ -768,7 +778,7 @@
     own = rows // ntp
     nx = ntp // 2
     vmem = pl.BlockSpec(memory_space=pltpu.VMEM)
-    hbm = pl.BlockSpec(memory_space=pl.ANY)
+    hbm = pl.BlockSpec(memory_space=pltpu.HBM)
     return pl.pallas_call(
         functools.partial(kernel, nz, ny, ntp),
         out_shape=jax.ShapeDtypeStruct((own, width), BF),
@@ -784,12 +794,12 @@
             pltpu.VMEM((2, HS), F32),
             pltpu.VMEM((1, W2), F32),
             pltpu.VMEM((1, width), F32),
-            pltpu.VMEM((nz * ny, 2 * half_f + half_f // 4, ff), BF),
-            pltpu.VMEM((nz * ny, half_f - half_f // 4, ff), BF),
+            pltpu.VMEM((nz * ny, 2 * half_f, ff), BF),
+            pltpu.VMEM((nz * ny, half_f, ff), BF),
             pltpu.VMEM((ntp, W2, width), BF),
             pltpu.VMEM((rows, width), BF),
-            pltpu.VMEM((ny, W2, W2), F32),
-            pltpu.VMEM((nz, W2, W2), F32),
+            pltpu.VMEM((ny, W2, W2), BF),
+            pltpu.VMEM((nz, W2, W2), BF),
             pltpu.VMEM((rows // CHUNK, W2, W2), F32),
             pltpu.VMEM((rows, W2), F32),
             pltpu.VMEM((rows, W2), F32),
@@ -802,7 +812,7 @@
             pltpu.VMEM((max(nx - 1, 1), own, width), BF),
             pltpu.VMEM((nx, own, width), BF),
             pltpu.VMEM((max(nx - 1, 1), own, width), BF),
-            pltpu.SemaphoreType.DMA((15,)),
+            pltpu.SemaphoreType.DMA((14,)),
             pltpu.SemaphoreType.DMA((8,)),
             pltpu.SemaphoreType.DMA((SEMS,)),
         ],

time: 89.9 us -> 81.9 us (0.911)
  Pallas kernels: 88.2 us -> 80.2 us
    pallas_call x1, Pallas kernels: 88.2 us -> 80.2 us  [per_device(): pl.pallas_call(functools.partial(kernel, nz, ny, ntp), out_shape=jax.Shap...]
where the time goes in v4:
time: 81.9 us; the launch traced here: 81.7 us
  Pallas kernels  80.2 us (98%)
  local copies, waits for them, and re-layouts  1.54 us (2%)
    pallas_call x1, Pallas kernels, per_device(): pl.pallas_call(functools.partial(kernel, nz, ny, ntp), out_shape=jax.Shap...  80.2 us

profile of v4, /device:TPU:1, one launch (start us, length us, event | category | flops | bytes accessed | tf_op | source)
XLA Modules:
  0.0 81.7 jit_solution(2121686098343145895)
XLA Ops:
  0.0 80.2 %layer.1 = bf16[24,2048]{1,0:T(8,128)(2,1)} custom-call(bf16[192,128]{1,0:T(8,128)(2,1)} %r_in.1, bf16[192,128]{1,0:T(8,128)(2,1)} %k_in.1, bf16[192,128]{1,0:T(8,128)(2,1)} %v_in.1, f32[192,128]{1,0:T(8,128)} %pre_in.1, f32[192,128]{1,0:T(8,128)} %lr_in.1, bf16[192,128]{1,0:T(8,128)(2,1)} %og_in.1, f32[2,64]{1,0:T(2,128)} %stw_in.1, f32[1,128]{1,0:T(1,128)} %bitcast.5, ...), custom_call_target="tpu_custom_call" | custom-call | tf_op jit(solution)/shard_map/layer/pallas_call | solution.py:782
  80.2 1.5 %copy.16 = bf16[24,2048]{1,0:T(8,128)(2,1)} copy(bf16[24,2048]{1,0:T(8,128)(2,1)} %layer.1) | data formatting | bytes 196608

commit v5 on v4

--- a/solution.py
+++ b/solution.py
@@ -116,7 +116,6 @@
         m["mb"] = jnp.where(incl, gram[W2:, :W2], 0.0)
         m["mk"] = jnp.where(incl, gram[W2:, W2:], 0.0)
         m["vs"] = m["v"].astype(BF)
-    yield
     for m in made:
         m["lkv"] = dot2(m["lk"], m["vs"])
         m["mkv"] = dot2(m["mk"], m["vs"])
@@ -135,6 +134,8 @@
             for m, h, x in zip(made, held, mid):
                 m["inv"] = m["inv"] + dot_halves(halves(x), h)
         size *= 2
+        if size == 8:
+            yield
     for m in made:
         m["tuv"] = dot3(m["inv"], jnp.concatenate([m["us"], m["lkv"]], axis=1))
     out = []
@@ -198,6 +199,7 @@
     got,
     pgot,
     comb,
+    early_sum,
     lsem,
     ssem,
     rsem,
@@ -406,18 +408,19 @@
     for s in range(1, half_ring):
         order += [-s, s]
     order += [half_ring]
-    far_halves = channel()
+    late = max(1, nz // 4)
+    far_early, far_late = channel(), channel()
     across = [
         Across(
             functools.partial(lambda step, yy, piece: gu_block(zof(step), yy, piece), step),
             yof,
             y_dev,
             GU,
-            gu.at[0:nz],
+            gu.at[0:late] if i >= nz - late else gu.at[0 : nz - late],
             gu.at[0:2],
-            far_halves,
+            far_late if i >= nz - late else far_early,
         )
-        for step in order
+        for i, step in enumerate(order)
     ]
     across_dn = Across(
         lambda yy, piece: dn_block(z, yy, piece), yof, y_dev, DN, dn.at[0], dn.at[0:2]
@@ -566,14 +569,15 @@
         mark(f"scan_z{s}")
         ring_ps.turn(s)
         mark(f"bulk{s}")
-        if s in (1, 2, 4, 6, 7):
-            turn_gu()
-            turn_dn(2)
-        else:
-            turn_dn(4)
-        y_push(2)
-        mark(f"yfwd{s}")
-        y_forward(2 if s % 2 == 0 else 1)
+        if s < half_ring:
+            if s in (1, 2, 4, 6, 7):
+                turn_gu()
+                turn_dn(2)
+            else:
+                turn_dn(4)
+            y_push(2)
+            mark(f"yfwd{s}")
+            y_forward(2 if s % 2 == 0 else 1)
         mark(f"calc{s}")
         if s == half_ring // 2:
             ow_middle()
@@ -594,9 +598,6 @@
     state = state_right + dot3(state_right, stacked(trans_left)) + state_left
     state = state + dot3(state, stacked(inside[:HS])) + inside[HS:]
 
-    turn_gu()
-    y_push(2)
-    turn_dn(1)
     mark("mech")
     seen = []
     for c in range(chunks):
@@ -616,20 +617,25 @@
         send(mx.at[tp], MX, mx_far[d - 1], x_dev(d))
     send(mx.at[tp], MX, mx_near, near)
     mark("exch_pump")
+    turn_dn(2)
     y_forward()
-    turn_dn(3)
+    turn_gu()
+    y_push(2)
+    turn_dn(2)
+    y_forward()
     mark("exch_far")
     for d in reversed(x_order):
         arrived(mx.at[0], mx_far[d - 1])
         send(mx.at[same_core(-d)], MX, mx_near, near)
     mark("exch_pump2")
+    turn_dn(2)
     y_forward()
-    turn_dn(3)
     mark("exch_near")
     arrived(mx.at[0:nx], mx_near)
     mark("exch_ow")
     ow_finish()
     mark("exch_pump3")
+    turn_dn(1)
     y_push(2)
     y_forward()
 
@@ -670,19 +676,42 @@
         y_push(2)
         y_forward()
         turn_dn()
-    mark("finish")
+    z_rows = ny * half_f
+
+    def gate_up(steps, at, wide):
+        x = jnp.concatenate(
+            [normed[:, pl.ds(pl.multiple_of(zof(t) * z_rows, z_rows), z_rows)] for t in steps],
+            axis=1,
+        )
+        sums = []
+        for first in (0, half_f):
+            w = [
+                gu[pl.ds(zof(t) * ny, ny), first : first + half_f, at : at + wide].reshape(
+                    z_rows, wide
+                )
+                for t in steps
+            ]
+            sums.append(dg(x, jnp.concatenate(w, axis=0)))
+        return sums
+
+    bands = [(at, min(256, ff - at)) for at in range(0, ff, 256)]
+    mark("finish_a")
     across[0].finish()
-
-    mark("gateup")
-    at = 0
-    while at < ff:
-        wide = min(256, ff - at)
-        x = normed[...]
-        gate = dg(x, gu[:, 0:half_f, at : at + wide].reshape(width, wide))
-        up = dg(x, gu[:, half_f : 2 * half_f, at : at + wide].reshape(width, wide))
+    mark("gateup_a")
+    for at, wide in bands:
+        gate, up = gate_up(order[: nz - late], at, wide)
+        early_sum[0, :, at : at + wide] = gate
+        early_sum[1, :, at : at + wide] = up
+        turn_dn()
+    mark("finish_b")
+    turn_dn(2)
+    across[-1].finish()
+    mark("gateup_b")
+    for at, wide in bands:
+        gate, up = gate_up(order[nz - late :], at, wide)
+        gate = gate + early_sum[0, :, at : at + wide]
+        up = up + early_sum[1, :, at : at + wide]
         hid[:, at : at + wide] = (gate / (1.0 + jnp.exp(-gate)) * up).astype(BF)
-        at += wide
-        turn_dn(2)
     mark("dnwait")
     turn_dn(4 * half_ring)
 
@@ -812,6 +841,7 @@
             pltpu.VMEM((max(nx - 1, 1), own, width), BF),
             pltpu.VMEM((nx, own, width), BF),
             pltpu.VMEM((max(nx - 1, 1), own, width), BF),
+            pltpu.VMEM((2, rows, ff), F32),
             pltpu.SemaphoreType.DMA((14,)),
             pltpu.SemaphoreType.DMA((8,)),
             pltpu.SemaphoreType.DMA((SEMS,)),

time: 81.9 us -> 80.4 us (0.982)
  Pallas kernels: 80.2 us -> 78.7 us
    pallas_call x1, Pallas kernels: 80.2 us -> 78.7 us  [per_device(): pl.pallas_call(functools.partial(kernel, nz, ny, ntp), out_shape=jax.Shap...]
where the time goes in v5:
time: 80.4 us; the launch traced here: 80.3 us
  Pallas kernels  78.7 us (98%)
  local copies, waits for them, and re-layouts  1.54 us (2%)
    pallas_call x1, Pallas kernels, per_device(): pl.pallas_call(functools.partial(kernel, nz, ny, ntp), out_shape=jax.Shap...  78.7 us

profile of v5, /device:TPU:1, one launch (start us, length us, event | category | flops | bytes accessed | tf_op | source)
XLA Modules:
  0.0 80.3 jit_solution(4572748209603691807)
XLA Ops:
  0.0 78.7 %layer.1 = bf16[24,2048]{1,0:T(8,128)(2,1)} custom-call(bf16[192,128]{1,0:T(8,128)(2,1)} %r_in.1, bf16[192,128]{1,0:T(8,128)(2,1)} %k_in.1, bf16[192,128]{1,0:T(8,128)(2,1)} %v_in.1, f32[192,128]{1,0:T(8,128)} %pre_in.1, f32[192,128]{1,0:T(8,128)} %lr_in.1, bf16[192,128]{1,0:T(8,128)(2,1)} %og_in.1, f32[2,64]{1,0:T(2,128)} %stw_in.1, f32[1,128]{1,0:T(1,128)} %bitcast.5, ...), custom_call_target="tpu_custom_call" | custom-call | tf_op jit(solution)/shard_map/layer/pallas_call | solution.py:811
  78.7 1.5 %copy.16 = bf16[24,2048]{1,0:T(8,128)(2,1)} copy(bf16[24,2048]{1,0:T(8,128)(2,1)} %layer.1) | data formatting | bytes 196608

commit v6 on v5

--- a/solution.py
+++ b/solution.py
@@ -570,11 +570,11 @@
         ring_ps.turn(s)
         mark(f"bulk{s}")
         if s < half_ring:
-            if s in (1, 2, 4, 6, 7):
+            if s in (1, 2, 4, 5, 7):
                 turn_gu()
                 turn_dn(2)
             else:
-                turn_dn(4)
+                turn_dn(3)
             y_push(2)
             mark(f"yfwd{s}")
             y_forward(2 if s % 2 == 0 else 1)

time: 80.4 us -> 79.6 us (0.990)
    pallas_call x1, Pallas kernels: 78.7 us -> 77.9 us  [per_device(): pl.pallas_call(functools.partial(kernel, nz, ny, ntp), out_shape=jax.Shap...]
where the time goes in v6:
time: 79.6 us; the launch traced here: 79.4 us
  Pallas kernels  77.9 us (98%)
  local copies, waits for them, and re-layouts  1.54 us (2%)
    pallas_call x1, Pallas kernels, per_device(): pl.pallas_call(functools.partial(kernel, nz, ny, ntp), out_shape=jax.Shap...  77.9 us

profile of v6, /device:TPU:1, one launch (start us, length us, event | category | flops | bytes accessed | tf_op | source)
XLA Modules:
  0.0 79.4 jit_solution(14680934950467894471)
XLA Ops:
  0.0 77.9 %layer.1 = bf16[24,2048]{1,0:T(8,128)(2,1)} custom-call(bf16[192,128]{1,0:T(8,128)(2,1)} %r_in.1, bf16[192,128]{1,0:T(8,128)(2,1)} %k_in.1, bf16[192,128]{1,0:T(8,128)(2,1)} %v_in.1, f32[192,128]{1,0:T(8,128)} %pre_in.1, f32[192,128]{1,0:T(8,128)} %lr_in.1, bf16[192,128]{1,0:T(8,128)(2,1)} %og_in.1, f32[2,64]{1,0:T(2,128)} %stw_in.1, f32[1,128]{1,0:T(1,128)} %bitcast.5, ...), custom_call_target="tpu_custom_call" | custom-call | tf_op jit(solution)/shard_map/layer/pallas_call | solution.py:811
  77.9 1.5 %copy.16 = bf16[24,2048]{1,0:T(8,128)(2,1)} copy(bf16[24,2048]{1,0:T(8,128)(2,1)} %layer.1) | data formatting | bytes 196608

commit v7 on v6

--- a/solution.py
+++ b/solution.py
@@ -17,7 +17,7 @@
 BF = jnp.bfloat16
 NN = (((1,), (0,)), ((), ()))
 NT = (((1,), (1,)), ((), ()))
-SEMS = 96
+SEMS = 92
 
 
 def dg(a, b, dims=NN):
@@ -617,11 +617,10 @@
         send(mx.at[tp], MX, mx_far[d - 1], x_dev(d))
     send(mx.at[tp], MX, mx_near, near)
     mark("exch_pump")
-    turn_dn(2)
-    y_forward()
     turn_gu()
     y_push(2)
-    turn_dn(2)
+    y_forward()
+    turn_dn(4)
     y_forward()
     mark("exch_far")
     for d in reversed(x_order):

time: 79.6 us -> 79.5 us (level)
  no operation moved by 1% of the time
where the time goes in v7:
time: 79.5 us; the launch traced here: 79.4 us
  Pallas kernels  77.8 us (98%)
  local copies, waits for them, and re-layouts  1.54 us (2%)
    pallas_call x1, Pallas kernels, per_device(): pl.pallas_call(functools.partial(kernel, nz, ny, ntp), out_shape=jax.Shap...  77.8 us

profile of v7, /device:TPU:1, one launch (start us, length us, event | category | flops | bytes accessed | tf_op | source)
XLA Modules:
  0.0 79.4 jit_solution(14853977006661638122)
XLA Ops:
  0.0 77.8 %layer.1 = bf16[24,2048]{1,0:T(8,128)(2,1)} custom-call(bf16[192,128]{1,0:T(8,128)(2,1)} %r_in.1, bf16[192,128]{1,0:T(8,128)(2,1)} %k_in.1, bf16[192,128]{1,0:T(8,128)(2,1)} %v_in.1, f32[192,128]{1,0:T(8,128)} %pre_in.1, f32[192,128]{1,0:T(8,128)} %lr_in.1, bf16[192,128]{1,0:T(8,128)(2,1)} %og_in.1, f32[2,64]{1,0:T(2,128)} %stw_in.1, f32[1,128]{1,0:T(1,128)} %bitcast.5, ...), custom_call_target="tpu_custom_call" | custom-call | tf_op jit(solution)/shard_map/layer/pallas_call | solution.py:810
  77.8 1.5 %copy.16 = bf16[24,2048]{1,0:T(8,128)(2,1)} copy(bf16[24,2048]{1,0:T(8,128)(2,1)} %layer.1) | data formatting | bytes 196608
